TPU v7x, 32 devices: a whole 2x2x4 slice. The times are simulated.
32 devices in a mesh: ep: 4 (over y, x), tp: 8 (over z, core).
Axes of the slice: x: 2, y: 2, z: 4, core: 2. Of those that a mesh axis runs over, the one named last changes fastest.
Arguments:
- query_heads: bfloat16 [1024, 2048], P('ep', 'tp'), may hold values from -60 to 60
- key_heads: bfloat16 [1024, 2048], P('ep', 'tp'), may hold values from -40.5 to 40.5
- value_heads: bfloat16 [1024, 2048], P('ep', 'tp'), may hold values from -6 to 6
- diff_lambda: float32 [16], P('tp'), may hold values from 0.3 to 0.8
- sub_gain: float32 [128], replicated, may hold values from 0.1 to 1.9
- out_weight: bfloat16 [2048, 4096], P('tp'), may hold values from -0.125 to 0.125
- routed_input: bfloat16 [1024, 4096], P('ep', 'tp'), may hold values from -40 to 40
- routes: int32 [1024, 2], P('ep'), may hold values from 0 to 3, all different within a row; in each aligned block of 256 rows (0 to 255, 256 to 511, ...) at most 256 rows name the same one
- route_weights: float32 [1024, 2], P('ep'), may hold values from 0.3 to 1.5
- expert_gate: bfloat16 [4, 4096, 4096], P('ep', None, 'tp'), may hold values from -0.09375 to 0.09375
- expert_up: bfloat16 [4, 4096, 4096], P('ep', None, 'tp'), may hold values from -0.09375 to 0.09375
- expert_down: bfloat16 [4, 4096, 4096], P('ep', 'tp'), may hold values from -0.09375 to 0.09375
- shared_gate: bfloat16 [4096, 2048], P(None, 'tp'), may hold values from -0.09375 to 0.09375
- shared_up: bfloat16 [4096, 2048], P(None, 'tp'), may hold values from -0.09375 to 0.09375
- shared_down: bfloat16 [2048, 4096], P('tp'), may hold values from -0.125 to 0.125
Outputs:
- mixer_output: bfloat16 [1024, 4096], P('ep', 'tp')
- routed_output: bfloat16 [1024, 4096], P('ep', 'tp')
Inputs may be any that keep to these rules, and one draw needn't show every extreme that they name: `routes`: each row names 2 different experts. In each aligned block of 256 rows no expert is named by more than 256 rows, a bound that some block reaches.
All inputs are finite; a program needn't handle non-finite values.
Results may differ from a plain program's by a relative error of at most 0.02.
Values may be sent and summed in bfloat16 or wider, within the bound.
A program may use at most 128 MiB of HBM per device.

v0:
```python
import functools

import jax
import jax.numpy as jnp
import numpy as np
from jax import lax
from jax.experimental import pallas as pl
from jax.experimental.pallas import tpu as pltpu
from jax.sharding import PartitionSpec as P

ROPE_BASE = 10000.0
NORM_EPS = 1e-06
MASKED = -1e30


def rotate(values, positions):
    half_width = values.shape[-1] // 2
    inverse_freq = ROPE_BASE ** (-jnp.arange(half_width, dtype=jnp.float32) / half_width)
    angles = positions.astype(jnp.float32)[:, None] * inverse_freq[None, :]
    angles = angles.reshape((angles.shape[0],) + (1,) * (values.ndim - 2) + (half_width,))
    cosine = jnp.cos(angles)
    sine_part = jnp.sin(angles)
    lower = values[..., :half_width]
    upper = values[..., half_width:]
    return jnp.concatenate(
        [lower * cosine - upper * sine_part, upper * cosine + lower * sine_part], axis=-1
    )


def mixer_terms(query_heads, key_heads, value_heads, diff_lambda, sub_gain, out_weight):
    row_count = query_heads.shape[0]
    local_heads = diff_lambda.shape[0]
    value_width = value_heads.shape[1] // local_heads
    key_width = query_heads.shape[1] // (2 * local_heads)
    score_scale = key_width ** (-0.5)
    offset = lax.axis_index("ep") * row_count
    positions = offset + jnp.arange(row_count, dtype=jnp.int32)
    last_row = offset + row_count - 1
    query_rot = rotate(
        query_heads.astype(jnp.float32).reshape(row_count, local_heads, 2, key_width), positions
    ).astype(jnp.bfloat16)
    queries = jnp.transpose(query_rot, (1, 2, 0, 3))
    key_rot = (
        rotate(
            key_heads.astype(jnp.float32).reshape(row_count, local_heads, 2, key_width), positions
        )
        .astype(jnp.bfloat16)
        .reshape(row_count, local_heads * 2 * key_width)
    )
    start_state = (
        jnp.full((local_heads, 2, row_count), MASKED, jnp.float32),
        jnp.zeros((local_heads, 2, row_count), jnp.float32),
        jnp.zeros((local_heads, 2, row_count, value_width), jnp.float32),
    )
    carried = start_state
    key_piece = lax.all_gather(key_rot, "ep", axis=0, tiled=True)
    value_piece = lax.all_gather(value_heads, "ep", axis=0, tiled=True)
    piece_rows = key_piece.shape[0]
    key_block = 512
    block_count = piece_rows // key_block
    key_blocks = key_piece.reshape(block_count, key_block, local_heads, 2, key_width)
    value_blocks = value_piece.reshape(block_count, key_block, local_heads, value_width)

    def block_step(running, block_item):
        key_rows, value_rows, block_index = block_item
        block_start = block_index * key_block

        def attend_block(partial_state):
            maxima, totals, weighted = partial_state
            key_positions = block_start + jnp.arange(key_block, dtype=jnp.int32)
            visible = key_positions[None, :] <= positions[:, None]
            scores = (
                jnp.einsum("hmqd,khmd->hmqk", queries, key_rows, preferred_element_type=jnp.float32)
                * score_scale
            )
            scores = jnp.where(visible, scores, MASKED)
            new_maxima = jnp.maximum(maxima, jnp.max(scores, axis=3))
            exp_weights = jnp.where(visible, jnp.exp(scores - new_maxima[..., None]), 0.0)
            shrink = jnp.exp(maxima - new_maxima)
            new_totals = totals * shrink + jnp.sum(exp_weights, axis=3)
            update = jnp.einsum(
                "hmqk,khw->hmqw",
                exp_weights.astype(jnp.bfloat16),
                value_rows,
                preferred_element_type=jnp.float32,
            )
            return (new_maxima, new_totals, weighted * shrink[..., None] + update)

        return (
            lax.cond(
                block_start <= last_row, attend_block, lambda partial_state: partial_state, running
            ),
            None,
        )

    carried, _ = lax.scan(
        block_step, carried, (key_blocks, value_blocks, jnp.arange(block_count, dtype=jnp.int32))
    )
    maxima, totals, weighted = carried
    attended = weighted / totals[..., None]
    mixed_heads = attended[:, 0] - diff_lambda[:, None, None] * attended[:, 1]
    normed = (
        mixed_heads
        * lax.rsqrt(jnp.mean(mixed_heads * mixed_heads, axis=2, keepdims=True) + NORM_EPS)
        * sub_gain
    )
    heads_out = jnp.transpose(normed.astype(jnp.bfloat16), (1, 0, 2)).reshape(
        row_count, local_heads * value_width
    )
    return jnp.dot(heads_out, out_weight, preferred_element_type=jnp.float32)


def expert_terms(
    routed_input, routes, expert_gate, expert_up, expert_down, shared_gate, shared_up, shared_down
):
    row_count, part_width = routed_input.shape
    top_count = routes.shape[1]
    local_experts = expert_gate.shape[0]
    groups = lax.axis_size("ep")
    experts = local_experts * groups
    capacity = 2 * row_count * top_count // experts
    copies = row_count * top_count
    flat_routes = routes.reshape(copies)
    onehot = (flat_routes[:, None] == jnp.arange(experts, dtype=jnp.int32)[None, :]).astype(
        jnp.int32
    )
    rank_within = jnp.sum((jnp.cumsum(onehot, axis=0) - onehot) * onehot, axis=1)
    slot_index = flat_routes * capacity + rank_within
    placer = (
        slot_index[:, None] == jnp.arange(experts * capacity, dtype=jnp.int32)[None, :]
    ).astype(jnp.bfloat16)
    token_slots = jnp.sum(placer.reshape(row_count, top_count, experts * capacity), axis=1)
    outgoing = jnp.dot(token_slots.T, routed_input, preferred_element_type=jnp.float32).astype(
        jnp.bfloat16
    )
    arrived = lax.all_to_all(
        outgoing.reshape(groups, local_experts * capacity, part_width),
        "ep",
        split_axis=0,
        concat_axis=0,
        tiled=True,
    )
    slot_count = groups * capacity
    slot_rows = jnp.transpose(
        arrived.reshape(groups, local_experts, capacity, part_width), (1, 0, 2, 3)
    ).reshape(local_experts, slot_count, part_width)
    slot_piece = lax.all_gather(slot_rows, "tp", axis=2, tiled=True)
    own_piece = lax.all_gather(routed_input[None], "tp", axis=2, tiled=True)
    own_rows = own_piece[0]
    gate_sum = jnp.einsum(
        "emc,ecf->emf", slot_piece, expert_gate, preferred_element_type=jnp.float32
    )
    up_sum = jnp.einsum("emc,ecf->emf", slot_piece, expert_up, preferred_element_type=jnp.float32)
    square_sum = jnp.sum(jnp.square(slot_piece.astype(jnp.float32)), axis=2)
    shared_gate_sum = jnp.dot(own_rows, shared_gate, preferred_element_type=jnp.float32)
    shared_up_sum = jnp.dot(own_rows, shared_up, preferred_element_type=jnp.float32)
    shared_square = jnp.sum(jnp.square(own_rows.astype(jnp.float32)), axis=1)
    full_width = expert_gate.shape[1]
    factor = lax.rsqrt(square_sum / full_width + NORM_EPS)[..., None]
    hidden = (jax.nn.silu(gate_sum * factor) * (up_sum * factor)).astype(jnp.bfloat16)
    shared_factor = lax.rsqrt(shared_square / full_width + NORM_EPS)[:, None]
    shared_hidden = (
        jax.nn.silu(shared_gate_sum * shared_factor) * (shared_up_sum * shared_factor)
    ).astype(jnp.bfloat16)
    shared_terms = jnp.dot(shared_hidden, shared_down, preferred_element_type=jnp.float32)
    routed_terms = jnp.einsum(
        "emf,efd->emd", hidden, expert_down, preferred_element_type=jnp.float32
    )
    routed_sum = lax.psum_scatter(
        routed_terms.astype(jnp.bfloat16), "tp", scatter_dimension=2, tiled=True
    ).astype(jnp.float32)
    return (routed_sum, shared_terms, placer)


def expert_finish(routed_sum, shared_sum, placer, route_weights):
    local_experts, slot_count, part_width = routed_sum.shape
    groups = lax.axis_size("ep")
    capacity = slot_count // groups
    leaving = jnp.transpose(
        routed_sum.astype(jnp.bfloat16).reshape(local_experts, groups, capacity, part_width),
        (1, 0, 2, 3),
    ).reshape(groups, local_experts * capacity, part_width)
    returned = lax.all_to_all(leaving, "ep", split_axis=0, concat_axis=0, tiled=True)
    copy_results = jnp.dot(
        placer,
        returned.reshape(groups * local_experts * capacity, part_width),
        preferred_element_type=jnp.float32,
    )
    row_count, top_count = route_weights.shape
    routed = jnp.sum(
        copy_results.reshape(row_count, top_count, part_width) * route_weights[:, :, None], axis=1
    )
    return (routed + shared_sum).astype(jnp.bfloat16)


def body(
    query_heads,
    key_heads,
    value_heads,
    diff_lambda,
    sub_gain,
    out_weight,
    routed_input,
    routes,
    route_weights,
    expert_gate,
    expert_up,
    expert_down,
    shared_gate,
    shared_up,
    shared_down,
):
    mixer_partial = mixer_terms(
        query_heads, key_heads, value_heads, diff_lambda, sub_gain, out_weight
    )
    routed_sum, shared_terms, placer = expert_terms(
        routed_input,
        routes,
        expert_gate,
        expert_up,
        expert_down,
        shared_gate,
        shared_up,
        shared_down,
    )
    mixer_sum, shared_sum = (
        lax.psum_scatter(
            mixer_partial.astype(jnp.bfloat16), "tp", scatter_dimension=1, tiled=True
        ).astype(jnp.float32),
        lax.psum_scatter(
            shared_terms.astype(jnp.bfloat16), "tp", scatter_dimension=1, tiled=True
        ).astype(jnp.float32),
    )
    return (
        mixer_sum.astype(jnp.bfloat16),
        expert_finish(routed_sum, shared_sum, placer, route_weights),
    )


MESH = pl.DeviceIdType.MESH
F32 = jnp.float32
BF16 = jnp.bfloat16
OWN, XB, YB, DB = 0, 1, 2, 3


def low(value):
    return value.astype(BF16)


def f32(value):
    return value.astype(F32)


def mm(left, right):
    return jnp.dot(left, right, preferred_element_type=F32)


def near_first(chips):
    rows = [sorted((s for s in range(chips) if s != z), key=lambda s: (abs(s - z), s if z < chips // 2 else -s)) for z in range(chips)]
    return [[row[j] for row in rows] for j in range(chips - 1)]


def far_first(chips):
    rows = []
    for z in range(chips):
        right = list(range(chips - 1, z, -1))
        left = list(range(0, z))
        first, second = (right, left) if z < chips // 2 else (left, right)
        row = []
        while first or second:
            if first:
                row.append(first.pop(0))
            if second:
                row.append(second.pop(0))
        rows.append(row)
    return [[row[j] for row in rows] for j in range(chips - 1)]


def layer_kernel(
    chips,
    q_ref,
    k_ref,
    v_ref,
    lam_ref,
    gain_ref,
    x_ref,
    routes_ref,
    rw_ref,
    tab_hbm,
    ow_hbm,
    gw_hbm,
    uw_hbm,
    dw_hbm,
    sg_hbm,
    su_hbm,
    sd_hbm,
    mix_ref,
    out_ref,
    xall,
    guw,
    dw,
    sgu,
    sd,
    ow,
    tab,
    acc,
    sacc,
    ssq,
    hid,
    shid,
    oacc,
    dsend,
    esend,
    lsend,
    late,
    din,
    xyin,
    zin,
    zout,
    macc,
    kv,
    qrot,
    sc_s,
    sc_p,
    sc_t,
    sc_o,
    ho,
    shtab,
    shcol,
    w_l,
    w_s,
    w_r,
    ag_s,
    ag_r,
    xy_s,
    xy_r,
    dr_s,
    dr_r,
    pt_s,
    pt_r,
    kv_s,
    kv_r,
    sh_s,
    sh_r,
    h_s,
    h_r,
    d_s,
    d_r,
    e_s,
    e_r,
    z_s,
    z_r,
):
    rows, part = x_ref.shape
    half = rows // 2
    wide = 2 * part
    hidden = gw_hbm.shape[1]
    shared = sg_hbm.shape[1]
    vwide = v_ref.shape[1]
    kwide = k_ref.shape[1]
    local_heads = lam_ref.shape[0]
    vd = vwide // local_heads
    qk = kwide // (2 * local_heads)
    e = lax.axis_index("ep")
    t = lax.axis_index("tp")
    z, c = t // 2, t % 2
    x, y = e % 2, e // 2
    pt = (e, t + 1 - 2 * c)
    xn = (e + 1 - 2 * x, t)
    yn = (e + 2 - 4 * y, t)
    zr = (e, t + 2)
    zl = (e, t - 2)
    has_r = z < chips - 1
    has_l = z > 0

    def chosen_by_z(column):
        return sum(order * (z == at).astype(jnp.int32) for at, order in enumerate(column))

    nears = [chosen_by_z(column) for column in near_first(chips)]
    fars = [chosen_by_z(column) for column in far_first(chips)] + [z]

    def remote(src, dst, send, recv, dev):
        pltpu.make_async_remote_copy(src, dst, send, recv, device_id=dev, device_id_type=MESH).start()

    def got(dst, recv):
        pltpu.make_async_remote_copy(dst, dst, recv, recv, device_id=pt, device_id_type=MESH).wait_recv()

    def sent(src, send):
        pltpu.make_async_remote_copy(src, src, send, send, device_id=pt, device_id_type=MESH).wait_send()

    def cols(index, width):
        return pl.ds(pl.multiple_of(index * width, width), width)

    loads = [
        pltpu.make_async_copy(gw_hbm, guw.at[:, pl.ds(0, hidden)], w_l.at[0]),
        pltpu.make_async_copy(uw_hbm, guw.at[:, pl.ds(hidden, hidden)], w_l.at[1]),
        pltpu.make_async_copy(sg_hbm, sgu.at[:, pl.ds(0, shared)], w_l.at[2]),
        pltpu.make_async_copy(su_hbm, sgu.at[:, pl.ds(shared, shared)], w_l.at[3]),
        pltpu.make_async_copy(tab_hbm.at[pl.ds(pl.multiple_of(e * rows, rows), rows), :], tab, w_l.at[4]),
    ]
    downs = [(ow_hbm, ow, vwide), (sd_hbm, sd, shared), (dw_hbm, dw, hidden)]
    for i, (src, dst, depth) in enumerate(downs):
        for p in range(chips):
            loads.append(
                pltpu.make_async_copy(
                    src.at[:, cols(2 * p + c, part)],
                    dst.at[cols(c, depth), pl.ds(p * part, part)],
                    w_l.at[5 + i * chips + p],
                )
            )
    loads[4].start()
    for i in list(range(4)) + list(range(5, len(loads))):
        loads[i].start()

    barrier = pltpu.get_barrier_semaphore()
    for dev in (pt, xn, yn):
        pl.semaphore_signal(barrier, inc=1, device_id=dev, device_id_type=MESH)

    @pl.when(has_r)
    def _():
        pl.semaphore_signal(barrier, inc=1, device_id=zr, device_id_type=MESH)

    @pl.when(has_l)
    def _():
        pl.semaphore_signal(barrier, inc=1, device_id=zl, device_id_type=MESH)

    pl.semaphore_wait(barrier, 3 + has_r.astype(jnp.int32) + has_l.astype(jnp.int32))

    def piece(block, s, core):
        return xall.at[block, :, cols(2 * s + core, part)]

    def z_forward(src, kind, block, s, right, left):
        @pl.when(right)
        def _():
            remote(src, piece(block, s, c), ag_s.at[kind, 0, s], ag_r.at[kind, s], zr)

        @pl.when(left)
        def _():
            remote(src, piece(block, s, c), ag_s.at[kind, 1, s], ag_r.at[kind, s], zl)

    def to_pair(src, block, s):
        remote(src, piece(block, s, c), pt_s.at[block, s], pt_r.at[block, s], pt)

    def to_xy(src, s):
        remote(src, piece(XB, s, c), xy_s.at[0, s], xy_r.at[0, s], xn)
        remote(src, piece(YB, s, c), xy_s.at[1, s], xy_r.at[1, s], yn)

    z_forward(x_ref, 0, OWN, z, has_r, has_l)
    to_xy(x_ref, z)
    to_pair(x_ref, OWN, z)
    xall[OWN, :, cols(t, part)] = x_ref[...]

    lane = lax.broadcasted_iota(jnp.int32, (rows, 128), 1)
    routes = routes_ref[...]
    weights = rw_ref[...]
    table = jnp.zeros((rows, 128), F32)
    for k in range(routes.shape[1]):
        table = table + jnp.where(routes[:, k : k + 1] == lane, weights[:, k : k + 1], 0.0)
    shtab[OWN] = table.T[:8, :]
    remote(shtab.at[OWN], shtab.at[XB], sh_s.at[0], sh_r.at[0], xn)
    remote(shtab.at[OWN], shtab.at[YB], sh_s.at[1], sh_r.at[1], yn)

    loads[4].wait()
    cosine, sine = tab[:, :128], tab[:, 128:]
    at_row = lax.broadcasted_iota(jnp.int32, (128, 128), 0)
    at_col = lax.broadcasted_iota(jnp.int32, (128, 128), 1)
    swapped = at_col + qk // 2 - qk * ((at_col // (qk // 2)) % 2)
    swap = jnp.where(at_row == swapped, 1.0, 0.0).astype(BF16)
    for i in range(kwide // 128):
        span = slice(i * 128, (i + 1) * 128)
        for src, dst in ((q_ref, qrot), (k_ref, None)):
            value = src[:, span]
            turned = low(f32(value) * cosine + mm(value, swap) * sine)
            if dst is None:
                kv[0:rows, span] = turned
            else:
                dst[:, span] = turned
    kv[0:rows, kwide:] = v_ref[...]

    def kv_rows(block, start, count):
        return kv.at[pl.ds(block * rows + start, count), :]

    remote(kv_rows(OWN, 0, rows), kv_rows(XB, 0, rows), kv_s.at[0], kv_r.at[0], xn)
    remote(kv_rows(OWN, 0, rows), kv_rows(YB, 0, rows), kv_s.at[1], kv_r.at[1], yn)

    for i, (src, dst, depth) in enumerate(downs):
        for p in range(chips):
            remote(
                src.at[:, cols(2 * p + 1 - c, part)],
                dst.at[cols(c, depth), pl.ds(p * part, part)],
                w_s.at[i, p],
                w_r.at[i, p],
                pt,
            )

    def chunk(block, s, first, weight, target, width):
        tiles = target.shape[-1] // width

        def tile(n, carry):
            span = cols(n, width)
            value = mm(xall[block, :, cols(s, wide)], weight[cols(s, wide), span])
            if not first:
                value = value + target[:, span]
            target[:, span] = value
            return carry

        lax.fori_loop(0, tiles, tile, 0)

    def squares(block, s, first):
        total = jnp.zeros((rows, 128), F32) if first else ssq[block]
        for i in range(wide // 128):
            value = f32(xall[block, :, pl.ds(pl.multiple_of(s * wide + i * 128, 128), 128)])
            total = total + value * value
        ssq[block] = total

    def expert_chunk(block, s, first):
        got(piece(block, s, 1 - c), pt_r.at[block, s])
        chunk(block, s, first, guw, acc.at[block], hidden)
        squares(block, s, first)

    def shared_chunk(s, first):
        chunk(OWN, s, first, sgu, sacc, 2 * shared)

    def activate(block, source, width, target, index):
        full = jnp.sum(ssq[block], axis=1, keepdims=True) / (chips * wide)
        factor = lax.rsqrt(full + NORM_EPS)
        gate = source[:, :width] * factor
        up = source[:, width:] * factor
        target[:, cols(c, width)] = low(gate / (1.0 + jnp.exp(-gate)) * up)
        mine = target.at[:, cols(c, width)]
        remote(mine, mine, h_s.at[index], h_r.at[index], pt)

    def own_arrival(s):
        got(piece(OWN, s, c), ag_r.at[0, s])
        src = piece(OWN, s, c)
        z_forward(src, 0, OWN, s, (s < z) & has_r, (s > z) & has_l)
        to_xy(src, s)
        to_pair(src, OWN, s)

    def side_arrival(s):
        for i, block in ((0, XB), (1, YB)):
            got(piece(block, s, c), xy_r.at[i, s])
            to_pair(piece(block, s, c), block, s)

    def far_half(s, i):
        return xall.at[DB, pl.ds(i * half, half), cols(2 * s + c, part)]

    def far_arrival(s):
        got(piece(DB, s, c), ag_r.at[1, s])
        src = piece(DB, s, c)
        z_forward(src, 1, DB, s, (s < z) & has_r, (s > z) & has_l)
        to_pair(src, DB, s)

    side_arrival(z)
    remote(xall.at[XB, pl.ds(0, half), cols(t, part)], far_half(z, 0), dr_s.at[0], dr_r.at[0], yn)
    remote(xall.at[YB, pl.ds(half, half), cols(t, part)], far_half(z, 1), dr_s.at[1], dr_r.at[1], xn)
    own_arrival(nears[0])
    loads[0].wait()
    loads[1].wait()
    expert_chunk(OWN, z, True)
    got(shtab.at[XB], sh_r.at[0])
    got(shtab.at[YB], sh_r.at[1])
    remote(shtab.at[XB], shtab.at[DB], sh_s.at[2], sh_r.at[2], yn)
    expert_chunk(OWN, nears[0], False)
    own_arrival(nears[1])
    loads[2].wait()
    loads[3].wait()
    shared_chunk(z, True)
    got(kv_rows(XB, 0, rows), kv_r.at[0])
    got(kv_rows(YB, 0, rows), kv_r.at[1])
    remote(kv_rows(XB, 0, half), kv_rows(DB, 0, half), kv_s.at[2], kv_r.at[2], yn)
    remote(kv_rows(YB, half, half), kv_rows(DB, half, half), kv_s.at[3], kv_r.at[3], xn)
    expert_chunk(OWN, nears[1], False)
    got(far_half(z, 0), dr_r.at[0])
    got(far_half(z, 1), dr_r.at[1])
    z_forward(piece(DB, z, c), 1, DB, z, has_r, has_l)
    to_pair(piece(DB, z, c), DB, z)
    own_arrival(nears[2])
    expert_chunk(XB, z, True)
    expert_chunk(YB, z, True)
    expert_chunk(OWN, nears[2], False)
    activate(OWN, acc.at[OWN], hidden, hid.at[OWN], OWN)
    expert_chunk(DB, z, True)
    got(kv_rows(DB, 0, half), kv_r.at[2])
    got(kv_rows(DB, half, half), kv_r.at[3])
    key_count = kv.shape[0]
    step_rows = 32
    ids = (e, xn[0], yn[0], xn[0] + yn[0] - e)

    def one_map(h, m):
        in_map = (lax.broadcasted_iota(jnp.int32, (rows, 128), 1) // qk) == m
        query = jnp.where(in_map, qrot[:, cols(h, 128)], jnp.zeros((rows, 128), BF16))
        sc_s[...] = lax.dot_general(
            query, kv[:, cols(h, 128)], (((1,), (1,)), ((), ())), preferred_element_type=F32
        )

        def soften(r, carry):
            at = pl.ds(pl.multiple_of(r * step_rows, step_rows), step_rows)
            key = lax.broadcasted_iota(jnp.int32, (step_rows, key_count), 1)
            which = key // rows
            group = jnp.where(
                which == 0, ids[0], jnp.where(which == 1, ids[1], jnp.where(which == 2, ids[2], ids[3]))
            )
            key_at = group * rows + key % rows
            query_at = (
                e * rows + r * step_rows + lax.broadcasted_iota(jnp.int32, (step_rows, key_count), 0)
            )
            scores = jnp.where(key_at <= query_at, sc_s[at, :] * (qk ** (-0.5)), MASKED)
            weight = jnp.exp(scores - jnp.max(scores, axis=1, keepdims=True))
            total = jnp.sum(weight, axis=1, keepdims=True)
            sc_p[at, :] = low(weight)
            sc_t[at, :] = jnp.broadcast_to(total, (step_rows, 128))
            return carry

        lax.fori_loop(0, rows // step_rows, soften, 0)
        return mm(sc_p[...], kv[:, pl.ds(pl.multiple_of(kwide + h * vd, 128), vd)]) / sc_t[...]

    def one_head(h):
        sc_o[...] = one_map(h, 0)
        mixed = sc_o[...] - lam_ref[h] * one_map(h, 1)
        scale = lax.rsqrt(jnp.mean(mixed * mixed, axis=1, keepdims=True) + NORM_EPS)
        ho[:, pl.ds(pl.multiple_of(c * vwide + h * vd, 128), vd)] = low(mixed * scale * gain_ref[...])

    for h in range(local_heads):
        one_head(h)
        if h == 0:
            for i in range(1, chips - 1):
                shared_chunk(nears[i - 1], False)
    mine = ho.at[:, cols(c, vwide)]
    remote(mine, mine, h_s.at[5], h_r.at[5], pt)
    shared_chunk(nears[chips - 2], False)
    activate(OWN, sacc, shared, shid, 4)
    for j in range(chips - 1):
        side_arrival(nears[j])
        far_arrival(nears[j])
        last = j == chips - 2
        if j == 0:
            for p in range(chips):
                loads[5 + p].wait()
                got(ow.at[cols(1 - c, vwide), pl.ds(p * part, part)], w_r.at[0, p])
            got(ho.at[:, cols(1 - c, vwide)], h_r.at[5])
            for p in range(chips):
                macc[:, pl.ds(p * part, part)] = mm(ho[...], ow[:, pl.ds(p * part, part)])
        if j == 1:
            for p in range(chips):
                loads[5 + chips + p].wait()
                loads[5 + 2 * chips + p].wait()
                got(sd.at[cols(1 - c, shared), pl.ds(p * part, part)], w_r.at[1, p])
                got(dw.at[cols(1 - c, hidden), pl.ds(p * part, part)], w_r.at[2, p])
            got(hid.at[OWN, :, cols(1 - c, hidden)], h_r.at[OWN])
            got(shid.at[:, cols(1 - c, shared)], h_r.at[4])
            got(shtab.at[DB], sh_r.at[2])
            row_id = lax.broadcasted_iota(jnp.int32, (8, rows), 0)
            for block in range(4):
                line = jnp.sum(jnp.where(row_id == e, shtab[block], 0.0), axis=0, keepdims=True)
                shcol[block] = jnp.broadcast_to(line, (128, rows)).T

            def own_down(p, carry):
                span = cols(p, part)
                oacc[:, span] = mm(hid[OWN], dw[:, span]) * shcol[OWN, :, 0:1] + mm(shid[...], sd[:, span])
                return carry

            lax.fori_loop(0, chips, own_down, 0)
        for block in (DB, XB, YB):
            expert_chunk(block, nears[j], False)
            if last:
                activate(block, acc.at[block], hidden, hid.at[block], block)

    def z_send(kind, j, p, value_of):
        upstream = ((p > z) & has_l) | ((p < z) & has_r)
        slot = zout.at[kind, j]

        @pl.when(upstream)
        def _():
            got(zin.at[kind, p], z_r.at[kind, p])
            zout[kind, j] = low(value_of() + f32(zin[kind, p]))

        @pl.when(jnp.logical_not(upstream))
        def _():
            zout[kind, j] = low(value_of())

        @pl.when(p > z)
        def _():
            remote(slot, zin.at[kind, p], z_s.at[kind, j], z_r.at[kind, p], zr)

        @pl.when((p < z) & (p != z - 1))
        def _():
            remote(slot, zin.at[kind, p], z_s.at[kind, j], z_r.at[kind, p], zl)

        @pl.when((p < z) & (p == z - 1))
        def _():
            remote(slot, zin.at[kind, chips], z_s.at[kind, j], z_r.at[kind, chips], zl)

    def z_finish(kind, value):
        target = (mix_ref, out_ref)[kind]

        @pl.when(has_l)
        def _():
            got(zin.at[kind, z], z_r.at[kind, z])

        @pl.when(has_r)
        def _():
            got(zin.at[kind, chips], z_r.at[kind, chips])

        @pl.when(has_l & has_r)
        def _():
            target[...] = low(value + f32(zin[kind, z]) + f32(zin[kind, chips]))

        @pl.when(jnp.logical_not(has_l))
        def _():
            target[...] = low(value + f32(zin[kind, chips]))

        @pl.when(jnp.logical_not(has_r))
        def _():
            target[...] = low(value + f32(zin[kind, z]))

    def mixer_send(j):
        p = fars[j]
        z_send(0, j, p, lambda: macc[:, cols(p, part)])

    edge = jnp.logical_not(has_l & has_r)

    @pl.when(edge)
    def _():
        for j in range(chips - 1):
            mixer_send(j)

    def down(block, p):
        return mm(hid[block], dw[:, cols(p, part)]) * shcol[block, :, 0:1]

    top, rest = pl.ds(0, half), pl.ds(half, half)
    got(hid.at[DB, :, cols(1 - c, hidden)], h_r.at[DB])
    for j in range(chips):
        span = cols(fars[j], part)
        dsend[:, span] = low(down(DB, fars[j]))
        remote(dsend.at[top, span], din.at[0, :, span], d_s.at[0, j], d_r.at[0, j], xn)
        remote(dsend.at[rest, span], din.at[1, :, span], d_s.at[1, j], d_r.at[1, j], yn)
    for i, block, now, later, dev in ((0, XB, 0, 1, xn), (1, YB, 1, 0, yn)):
        got(hid.at[block, :, cols(1 - c, hidden)], h_r.at[block])
        now_rows = slice(now * half, (now + 1) * half)
        late_rows = slice(later * half, (later + 1) * half)
        for j in range(chips):
            span = cols(fars[j], part)
            value = down(block, fars[j])
            esend[i, :, span] = low(value[now_rows])
            late[i, :, span] = value[late_rows]
            remote(
                esend.at[i, :, span],
                xyin.at[i, pl.ds(now * half, half), span],
                e_s.at[i, 0, j],
                e_r.at[i, 0, j],
                dev,
            )
    for j in range(chips):
        span = cols(fars[j], part)
        for i, block, now, later, dev in ((0, XB, 0, 1, xn), (1, YB, 1, 0, yn)):
            got(din.at[1 - i, :, span], d_r.at[1 - i, j])
            lsend[i, :, span] = low(late[i, :, span] + f32(din[1 - i, :, span]))
            remote(
                lsend.at[i, :, span],
                xyin.at[i, pl.ds(later * half, half), span],
                e_s.at[i, 1, j],
                e_r.at[i, 1, j],
                dev,
            )

    @pl.when(jnp.logical_not(edge))
    def _():
        for j in range(chips - 1):
            mixer_send(j)

    z_finish(0, macc[:, cols(z, part)])

    for j in range(chips):
        p = fars[j]
        span = cols(p, part)
        for i, now, later in ((0, 0, 1), (1, 1, 0)):
            got(xyin.at[i, pl.ds(now * half, half), span], e_r.at[i, 0, j])
            got(xyin.at[i, pl.ds(later * half, half), span], e_r.at[i, 1, j])

        def total():
            return oacc[:, span] + f32(xyin[0, :, span]) + f32(xyin[1, :, span])

        if j < chips - 1:
            z_send(1, j, p, total)
        else:
            z_finish(1, total())

    for kind, block in ((0, OWN), (1, DB)):
        for s in range(chips):

            @pl.when(has_r & (s <= z))
            def _():
                sent(piece(block, s, c), ag_s.at[kind, 0, s])

            @pl.when(has_l & (s >= z))
            def _():
                sent(piece(block, s, c), ag_s.at[kind, 1, s])

    for s in range(chips):
        for i in range(2):
            sent(piece(OWN, s, c), xy_s.at[i, s])
        for block in range(4):
            sent(piece(block, s, c), pt_s.at[block, s])
    for i in range(2):
        sent(far_half(z, i), dr_s.at[i])
        sent(kv_rows(OWN, 0, rows), kv_s.at[i])
        sent(kv_rows(OWN, 0, half), kv_s.at[2 + i])
    for i in range(3):
        sent(shtab.at[OWN], sh_s.at[i])
        for p in range(chips):
            src, dst, depth = downs[i]
            sent(dst.at[cols(c, depth), pl.ds(p * part, part)], w_s.at[i, p])
    for block in range(4):
        sent(hid.at[block, :, cols(c, hidden)], h_s.at[block])
    sent(shid.at[:, cols(c, shared)], h_s.at[4])
    sent(ho.at[:, cols(c, vwide)], h_s.at[5])
    for i in range(2):
        for j in range(chips):
            sent(dsend.at[top, pl.ds(j * part, part)], d_s.at[i, j])
            sent(esend.at[i, :, pl.ds(j * part, part)], e_s.at[i, 0, j])
            sent(lsend.at[i, :, pl.ds(j * part, part)], e_s.at[i, 1, j])
        for j in range(chips - 1):
            sent(zout.at[i, j], z_s.at[i, j])


def rotation_table(positions, key_width):
    half_width = key_width // 2
    freq = np.float32(ROPE_BASE) ** (-np.arange(half_width, dtype=np.float32) / np.float32(half_width))
    angles = np.arange(positions, dtype=np.float32)[:, None] * freq.astype(np.float32)[None, :]
    angles = angles.astype(np.float64)
    cosine, sine = np.cos(angles), np.sin(angles)
    copies = 128 // key_width
    cosine = np.tile(np.concatenate([cosine, cosine], axis=1), (1, copies))
    sine = np.tile(np.concatenate([-sine, sine], axis=1), (1, copies))
    return np.concatenate([cosine, sine], axis=1).astype(np.float32)


def kernel_body(
    query_heads,
    key_heads,
    value_heads,
    diff_lambda,
    sub_gain,
    out_weight,
    routed_input,
    routes,
    route_weights,
    expert_gate,
    expert_up,
    expert_down,
    shared_gate,
    shared_up,
    shared_down,
):
    rows, part = routed_input.shape
    chips = lax.axis_size("tp") // 2
    groups = lax.axis_size("ep")
    gate, up, down = expert_gate[0], expert_up[0], expert_down[0]
    width, hidden = gate.shape
    shared = shared_gate.shape[1]
    kwide, vwide = key_heads.shape[1], value_heads.shape[1]
    local_heads = diff_lambda.shape[0]
    half, mine = rows // 2, width // 2
    table = jnp.asarray(rotation_table(groups * rows, kwide // (2 * local_heads)))
    vmem = pl.BlockSpec(memory_space=pltpu.VMEM)
    smem = pl.BlockSpec(memory_space=pltpu.SMEM)
    hbm = pl.BlockSpec(memory_space=pl.ANY)
    dma = pltpu.SemaphoreType.DMA
    out = jax.ShapeDtypeStruct((rows, part), BF16)
    return pl.pallas_call(
        functools.partial(layer_kernel, chips),
        out_shape=(out, out),
        in_specs=[vmem, vmem, vmem, smem, vmem, vmem, vmem, vmem] + [hbm] * 8,
        out_specs=(vmem, vmem),
        scratch_shapes=[
            pltpu.VMEM((groups, rows, width), BF16),
            pltpu.VMEM((width, 2 * hidden), BF16),
            pltpu.VMEM((2 * hidden, mine), BF16),
            pltpu.VMEM((width, 2 * shared), BF16),
            pltpu.VMEM((2 * shared, mine), BF16),
            pltpu.VMEM((2 * vwide, mine), BF16),
            pltpu.VMEM((rows, 256), F32),
            pltpu.VMEM((groups, rows, 2 * hidden), F32),
            pltpu.VMEM((rows, 2 * shared), F32),
            pltpu.VMEM((groups, rows, 128), F32),
            pltpu.VMEM((groups, rows, 2 * hidden), BF16),
            pltpu.VMEM((rows, 2 * shared), BF16),
            pltpu.VMEM((rows, mine), F32),
            pltpu.VMEM((rows, mine), BF16),
            pltpu.VMEM((2, half, mine), BF16),
            pltpu.VMEM((2, half, mine), BF16),
            pltpu.VMEM((2, half, mine), F32),
            pltpu.VMEM((2, half, mine), BF16),
            pltpu.VMEM((2, rows, mine), BF16),
            pltpu.VMEM((2, chips + 1, rows, part), BF16),
            pltpu.VMEM((2, chips - 1, rows, part), BF16),
            pltpu.VMEM((rows, mine), F32),
            pltpu.VMEM((groups * rows, kwide + vwide), BF16),
            pltpu.VMEM((rows, kwide), BF16),
            pltpu.VMEM((rows, groups * rows), F32),
            pltpu.VMEM((rows, groups * rows), BF16),
            pltpu.VMEM((rows, 128), F32),
            pltpu.VMEM((rows, 128), F32),
            pltpu.VMEM((rows, 2 * vwide), BF16),
            pltpu.VMEM((groups, 8, rows), F32),
            pltpu.VMEM((groups, rows, 128), F32),
            dma((5 + 3 * chips,)),
            dma((3, chips)),
            dma((3, chips)),
            dma((2, 2, chips)),
            dma((2, chips)),
            dma((2, chips)),
            dma((2, chips)),
            dma((2,)),
            dma((2,)),
            dma((4, chips)),
            dma((4, chips)),
            dma((4,)),
            dma((4,)),
            dma((3,)),
            dma((3,)),
            dma((6,)),
            dma((6,)),
            dma((2, chips)),
            dma((2, chips)),
            dma((2, 2, chips)),
            dma((2, 2, chips)),
            dma((2, chips - 1)),
            dma((2, chips + 1)),
        ],
        compiler_params=pltpu.CompilerParams(
            collective_id=0, has_side_effects=True, vmem_limit_bytes=67043328
        ),
        name="layer",
    )(
        query_heads,
        key_heads,
        value_heads,
        diff_lambda,
        sub_gain[None, :],
        routed_input,
        routes,
        route_weights,
        table,
        out_weight,
        gate,
        up,
        down,
        shared_gate,
        shared_up,
        shared_down,
    )


def solution(mesh):
    dense = mesh.shape["ep"] == 4 and mesh.shape["tp"] == 8

    def chosen(*arguments):
        fits = dense and arguments[9].shape[0] == 1 and arguments[6].shape[0] % 32 == 0
        return (kernel_body if fits else body)(*arguments)

    placed = (
        P("ep", "tp"),
        P("ep", "tp"),
        P("ep", "tp"),
        P("tp"),
        P(),
        P("tp", None),
        P("ep", "tp"),
        P("ep", None),
        P("ep", None),
        P("ep", None, "tp"),
        P("ep", None, "tp"),
        P("ep", "tp", None),
        P(None, "tp"),
        P(None, "tp"),
        P("tp", None),
    )
    return jax.shard_map(
        chosen, mesh=mesh, in_specs=placed, out_specs=(P("ep", "tp"), P("ep", "tp")), check_vma=False
    )
```

profile of v0, /device:TPU:0, one launch (start us, length us, event | category | flops | bytes accessed | tf_op | source)
XLA Modules:
  0.0 127.4 jit_solution(6706789528233075378)
XLA Ops:
  0.6 1.5 %copy.18.routes_ref = s32[256,2]{1,0:T(8,128)} copy(s32[256,2]{0,1:T(2,128)} %param.23) | data formatting | bytes 4096 | tf_op args[7]
  2.1 1.5 %copy.19.rw_ref = f32[256,2]{1,0:T(8,128)} copy(f32[256,2]{0,1:T(2,128)} %param.24) | data formatting | bytes 4096 | tf_op args[8]
  3.6 120.5 %layer.1 = (bf16[256,512]{1,0:T(8,128)(2,1)}, bf16[256,512]{1,0:T(8,128)(2,1)}) custom-call(bf16[256,256]{1,0:T(8,128)(2,1)} %q_ref.1, bf16[256,256]{1,0:T(8,128)(2,1)} %k_ref.1, bf16[256,256]{1,0:T(8,128)(2,1)} %v_ref.1, f32[2]{0:T(128)} %lam_ref.1, f32[1,128]{1,0:T(1,128)} %bitcast.7, bf16[256,512]{1,0:T(8,128)(2,1)} %x_ref.1, s32[256,2]{1,0:T(8,128)} %copy.18.routes_ref, ...), custom_call_target="tpu_custom_call" | custom-call | tf_op jit(solution)/shard_map/layer/pallas_call | solution.py:871
  124.1 1.7 %copy.22 = bf16[256,512]{1,0:T(8,128)(2,1)} copy(bf16[256,512]{1,0:T(8,128)(2,1)} %get-tuple-element.4) | data formatting | bytes 524288
  125.7 1.7 %copy.23 = bf16[256,512]{1,0:T(8,128)(2,1)} copy(bf16[256,512]{1,0:T(8,128)(2,1)} %get-tuple-element.5) | data formatting | bytes 524288
where the time goes:
time: 128 us; the launch traced here: 127 us
  Pallas kernels  120 us (94%)
  local copies, waits for them, and re-layouts  6.29 us (5%)
    pallas_call x1, Pallas kernels, kernel_body(): pl.pallas_call(functools.partial(layer_kernel, chips), out_shape=(out, ou...  120 us
    unnamed x4, local copies, waits for them, and re-layouts  6.29 us

commit v1 on v0

--- a/solution.py
+++ b/solution.py
@@ -429,34 +429,45 @@
     def piece(block, s, core):
         return xall.at[block, :, cols(2 * s + core, part)]
 
-    def z_forward(src, kind, block, s, right, left):
+    def halved(block, s, h):
+        return xall.at[block, pl.ds(h * half, half), cols(2 * s + c, part)]
+
+    def z_forward(src, kind, block, s, h, right, left):
         @pl.when(right)
         def _():
-            remote(src, piece(block, s, c), ag_s.at[kind, 0, s], ag_r.at[kind, s], zr)
+            remote(src, halved(block, s, h), ag_s.at[kind, 0, s, h], ag_r.at[kind, s, h], zr)
 
         @pl.when(left)
         def _():
-            remote(src, piece(block, s, c), ag_s.at[kind, 1, s], ag_r.at[kind, s], zl)
+            remote(src, halved(block, s, h), ag_s.at[kind, 1, s, h], ag_r.at[kind, s, h], zl)
 
     def to_pair(src, block, s):
         remote(src, piece(block, s, c), pt_s.at[block, s], pt_r.at[block, s], pt)
 
-    def to_xy(src, s):
-        remote(src, piece(XB, s, c), xy_s.at[0, s], xy_r.at[0, s], xn)
-        remote(src, piece(YB, s, c), xy_s.at[1, s], xy_r.at[1, s], yn)
-
-    z_forward(x_ref, 0, OWN, z, has_r, has_l)
-    to_xy(x_ref, z)
+    def to_xy(s):
+        remote(piece(OWN, s, c), piece(XB, s, c), xy_s.at[0, s], xy_r.at[0, s], xn)
+        remote(piece(OWN, s, c), piece(YB, s, c), xy_s.at[1, s], xy_r.at[1, s], yn)
+
+    def own_half(i, order):
+        h = order if i == 0 else 1 - order
+        block, dev = ((XB, xn), (YB, yn))[i]
+        slot = z if order == 0 else chips
+        remote(x_ref.at[pl.ds(h * half, half), :], halved(block, z, h), xy_s.at[i, slot], xy_r.at[i, slot], dev)
+
+    for h in range(2):
+        z_forward(x_ref.at[pl.ds(h * half, half), :], 0, OWN, z, h, has_r, has_l)
+    own_half(0, 0)
+    own_half(1, 0)
     to_pair(x_ref, OWN, z)
     xall[OWN, :, cols(t, part)] = x_ref[...]
 
-    lane = lax.broadcasted_iota(jnp.int32, (rows, 128), 1)
+    expert_id = lax.broadcasted_iota(jnp.int32, (8, rows), 0)
     routes = routes_ref[...]
     weights = rw_ref[...]
-    table = jnp.zeros((rows, 128), F32)
-    for k in range(routes.shape[1]):
-        table = table + jnp.where(routes[:, k : k + 1] == lane, weights[:, k : k + 1], 0.0)
-    shtab[OWN] = table.T[:8, :]
+    table = jnp.zeros((8, rows), F32)
+    for k in range(routes.shape[0]):
+        table = table + jnp.where(routes[k : k + 1, :] == expert_id, weights[k : k + 1, :], 0.0)
+    shtab[OWN] = table
     remote(shtab.at[OWN], shtab.at[XB], sh_s.at[0], sh_r.at[0], xn)
     remote(shtab.at[OWN], shtab.at[YB], sh_s.at[1], sh_r.at[1], yn)
 
@@ -483,7 +494,11 @@
     remote(kv_rows(OWN, 0, rows), kv_rows(XB, 0, rows), kv_s.at[0], kv_r.at[0], xn)
     remote(kv_rows(OWN, 0, rows), kv_rows(YB, 0, rows), kv_s.at[1], kv_r.at[1], yn)
 
-    for i, (src, dst, depth) in enumerate(downs):
+    own_half(0, 1)
+    own_half(1, 1)
+
+    def give_down(i):
+        src, dst, depth = downs[i]
         for p in range(chips):
             remote(
                 src.at[:, cols(2 * p + 1 - c, part)],
@@ -530,57 +545,80 @@
         mine = target.at[:, cols(c, width)]
         remote(mine, mine, h_s.at[index], h_r.at[index], pt)
 
-    def own_arrival(s):
-        got(piece(OWN, s, c), ag_r.at[0, s])
-        src = piece(OWN, s, c)
-        z_forward(src, 0, OWN, s, (s < z) & has_r, (s > z) & has_l)
-        to_xy(src, s)
-        to_pair(src, OWN, s)
+    def z_arrival(kind, s, h):
+        block = (OWN, DB)[kind]
+        got(halved(block, s, h), ag_r.at[kind, s, h])
+        z_forward(halved(block, s, h), kind, block, s, h, (s < z) & has_r, (s > z) & has_l)
+        if h == 1:
+            to_pair(piece(block, s, c), block, s)
 
     def side_arrival(s):
         for i, block in ((0, XB), (1, YB)):
             got(piece(block, s, c), xy_r.at[i, s])
             to_pair(piece(block, s, c), block, s)
 
-    def far_half(s, i):
-        return xall.at[DB, pl.ds(i * half, half), cols(2 * s + c, part)]
-
-    def far_arrival(s):
-        got(piece(DB, s, c), ag_r.at[1, s])
-        src = piece(DB, s, c)
-        z_forward(src, 1, DB, s, (s < z) & has_r, (s > z) & has_l)
-        to_pair(src, DB, s)
-
-    side_arrival(z)
-    remote(xall.at[XB, pl.ds(0, half), cols(t, part)], far_half(z, 0), dr_s.at[0], dr_r.at[0], yn)
-    remote(xall.at[YB, pl.ds(half, half), cols(t, part)], far_half(z, 1), dr_s.at[1], dr_r.at[1], xn)
-    own_arrival(nears[0])
+    middle = has_l & has_r
+
+    def at_middle(work):
+        @pl.when(middle)
+        def _():
+            work()
+
+    def at_edge(work):
+        @pl.when(jnp.logical_not(middle))
+        def _():
+            work()
+
+    def arrivals(kind, *orders):
+        for h in range(2):
+            for j in orders:
+                z_arrival(kind, nears[j], h)
+
+    got(halved(XB, z, 0), xy_r.at[0, z])
+    got(halved(YB, z, 1), xy_r.at[1, z])
+    remote(halved(XB, z, 0), halved(DB, z, 0), dr_s.at[0], dr_r.at[0], yn)
+    remote(halved(YB, z, 1), halved(DB, z, 1), dr_s.at[1], dr_r.at[1], xn)
+    at_middle(lambda: arrivals(0, 0, 1))
+    at_edge(lambda: arrivals(0, 0))
     loads[0].wait()
     loads[1].wait()
     expert_chunk(OWN, z, True)
-    got(shtab.at[XB], sh_r.at[0])
-    got(shtab.at[YB], sh_r.at[1])
-    remote(shtab.at[XB], shtab.at[DB], sh_s.at[2], sh_r.at[2], yn)
-    expert_chunk(OWN, nears[0], False)
-    own_arrival(nears[1])
-    loads[2].wait()
-    loads[3].wait()
-    shared_chunk(z, True)
     got(kv_rows(XB, 0, rows), kv_r.at[0])
     got(kv_rows(YB, 0, rows), kv_r.at[1])
     remote(kv_rows(XB, 0, half), kv_rows(DB, 0, half), kv_s.at[2], kv_r.at[2], yn)
     remote(kv_rows(YB, half, half), kv_rows(DB, half, half), kv_s.at[3], kv_r.at[3], xn)
+    got(shtab.at[XB], sh_r.at[0])
+    got(shtab.at[YB], sh_r.at[1])
+    remote(shtab.at[XB], shtab.at[DB], sh_s.at[2], sh_r.at[2], yn)
+    to_xy(nears[0])
+    at_middle(lambda: to_xy(nears[1]))
+    got(halved(XB, z, 1), xy_r.at[0, chips])
+    got(halved(YB, z, 0), xy_r.at[1, chips])
+    to_pair(piece(XB, z, c), XB, z)
+    to_pair(piece(YB, z, c), YB, z)
+    at_middle(lambda: arrivals(0, 2))
+    at_edge(lambda: arrivals(0, 1))
+    at_middle(lambda: to_xy(nears[2]))
+    at_edge(lambda: to_xy(nears[1]))
+    give_down(0)
+    expert_chunk(OWN, nears[0], False)
+    loads[2].wait()
+    loads[3].wait()
+    shared_chunk(z, True)
+    got(halved(DB, z, 0), dr_r.at[0])
+    got(halved(DB, z, 1), dr_r.at[1])
+    for h in range(2):
+        z_forward(halved(DB, z, h), 1, DB, z, h, has_r, has_l)
+    to_pair(piece(DB, z, c), DB, z)
+
+    def last_own():
+        arrivals(0, 2)
+        to_xy(nears[2])
+
+    at_edge(last_own)
+    give_down(1)
+    give_down(2)
     expert_chunk(OWN, nears[1], False)
-    got(far_half(z, 0), dr_r.at[0])
-    got(far_half(z, 1), dr_r.at[1])
-    z_forward(piece(DB, z, c), 1, DB, z, has_r, has_l)
-    to_pair(piece(DB, z, c), DB, z)
-    own_arrival(nears[2])
-    expert_chunk(XB, z, True)
-    expert_chunk(YB, z, True)
-    expert_chunk(OWN, nears[2], False)
-    activate(OWN, acc.at[OWN], hidden, hid.at[OWN], OWN)
-    expert_chunk(DB, z, True)
     got(kv_rows(DB, 0, half), kv_r.at[2])
     got(kv_rows(DB, half, half), kv_r.at[3])
     key_count = kv.shape[0]
@@ -615,57 +653,25 @@
         lax.fori_loop(0, rows // step_rows, soften, 0)
         return mm(sc_p[...], kv[:, pl.ds(pl.multiple_of(kwide + h * vd, 128), vd)]) / sc_t[...]
 
-    def one_head(h):
+    for h in range(local_heads):
         sc_o[...] = one_map(h, 0)
+        at_middle(lambda: [z_arrival(1, nears[j], h) for j in (0, 1)])
         mixed = sc_o[...] - lam_ref[h] * one_map(h, 1)
         scale = lax.rsqrt(jnp.mean(mixed * mixed, axis=1, keepdims=True) + NORM_EPS)
         ho[:, pl.ds(pl.multiple_of(c * vwide + h * vd, 128), vd)] = low(mixed * scale * gain_ref[...])
-
-    for h in range(local_heads):
-        one_head(h)
-        if h == 0:
-            for i in range(1, chips - 1):
-                shared_chunk(nears[i - 1], False)
     mine = ho.at[:, cols(c, vwide)]
     remote(mine, mine, h_s.at[5], h_r.at[5], pt)
-    shared_chunk(nears[chips - 2], False)
-    activate(OWN, sacc, shared, shid, 4)
-    for j in range(chips - 1):
-        side_arrival(nears[j])
-        far_arrival(nears[j])
-        last = j == chips - 2
-        if j == 0:
-            for p in range(chips):
-                loads[5 + p].wait()
-                got(ow.at[cols(1 - c, vwide), pl.ds(p * part, part)], w_r.at[0, p])
-            got(ho.at[:, cols(1 - c, vwide)], h_r.at[5])
-            for p in range(chips):
-                macc[:, pl.ds(p * part, part)] = mm(ho[...], ow[:, pl.ds(p * part, part)])
-        if j == 1:
-            for p in range(chips):
-                loads[5 + chips + p].wait()
-                loads[5 + 2 * chips + p].wait()
-                got(sd.at[cols(1 - c, shared), pl.ds(p * part, part)], w_r.at[1, p])
-                got(dw.at[cols(1 - c, hidden), pl.ds(p * part, part)], w_r.at[2, p])
-            got(hid.at[OWN, :, cols(1 - c, hidden)], h_r.at[OWN])
-            got(shid.at[:, cols(1 - c, shared)], h_r.at[4])
-            got(shtab.at[DB], sh_r.at[2])
-            row_id = lax.broadcasted_iota(jnp.int32, (8, rows), 0)
-            for block in range(4):
-                line = jnp.sum(jnp.where(row_id == e, shtab[block], 0.0), axis=0, keepdims=True)
-                shcol[block] = jnp.broadcast_to(line, (128, rows)).T
-
-            def own_down(p, carry):
-                span = cols(p, part)
-                oacc[:, span] = mm(hid[OWN], dw[:, span]) * shcol[OWN, :, 0:1] + mm(shid[...], sd[:, span])
-                return carry
-
-            lax.fori_loop(0, chips, own_down, 0)
-        for block in (DB, XB, YB):
-            expert_chunk(block, nears[j], False)
-            if last:
-                activate(block, acc.at[block], hidden, hid.at[block], block)
-
+    at_edge(lambda: arrivals(1, 0))
+    side_arrival(nears[0])
+    expert_chunk(XB, z, True)
+    expert_chunk(YB, z, True)
+    for p in range(chips):
+        loads[5 + p].wait()
+        got(ow.at[cols(1 - c, vwide), pl.ds(p * part, part)], w_r.at[0, p])
+    got(ho.at[:, cols(1 - c, vwide)], h_r.at[5])
+    for j in range(chips):
+        span = cols(fars[j], part)
+        macc[:, span] = mm(ho[...], ow[:, span])
     def z_send(kind, j, p, value_of):
         upstream = ((p > z) & has_l) | ((p < z) & has_r)
         slot = zout.at[kind, j]
@@ -718,63 +724,76 @@
         p = fars[j]
         z_send(0, j, p, lambda: macc[:, cols(p, part)])
 
-    edge = jnp.logical_not(has_l & has_r)
-
-    @pl.when(edge)
-    def _():
-        for j in range(chips - 1):
-            mixer_send(j)
+    at_edge(lambda: [mixer_send(j) for j in range(chips - 1)])
+    at_middle(lambda: arrivals(1, 2))
+    expert_chunk(DB, z, True)
+    expert_chunk(OWN, nears[2], False)
+    activate(OWN, acc.at[OWN], hidden, hid.at[OWN], OWN)
+    for j in range(chips - 1):
+        shared_chunk(nears[j], False)
+    activate(OWN, sacc, shared, shid, 4)
+    for block in (XB, YB, DB):
+        expert_chunk(block, nears[0], False)
+    at_edge(lambda: arrivals(1, 1))
+    side_arrival(nears[1])
+    for p in range(chips):
+        loads[5 + chips + p].wait()
+        loads[5 + 2 * chips + p].wait()
+        got(sd.at[cols(1 - c, shared), pl.ds(p * part, part)], w_r.at[1, p])
+        got(dw.at[cols(1 - c, hidden), pl.ds(p * part, part)], w_r.at[2, p])
+    got(hid.at[OWN, :, cols(1 - c, hidden)], h_r.at[OWN])
+    got(shid.at[:, cols(1 - c, shared)], h_r.at[4])
+    got(shtab.at[DB], sh_r.at[2])
+    for block in range(4):
+        line = jnp.sum(jnp.where(expert_id == e, shtab[block], 0.0), axis=0, keepdims=True)
+        shcol[block] = jnp.broadcast_to(line, (128, rows)).T
+
+    def own_down(p, carry):
+        span = cols(p, part)
+        oacc[:, span] = mm(hid[OWN], dw[:, span]) * shcol[OWN, :, 0:1] + mm(shid[...], sd[:, span])
+        return carry
+
+    for block in (XB, YB, DB):
+        expert_chunk(block, nears[1], False)
+    lax.fori_loop(0, chips, own_down, 0)
+    at_edge(lambda: arrivals(1, 2))
+    side_arrival(nears[2])
+    for block in (DB, XB, YB):
+        expert_chunk(block, nears[2], False)
+        activate(block, acc.at[block], hidden, hid.at[block], block)
 
     def down(block, p):
         return mm(hid[block], dw[:, cols(p, part)]) * shcol[block, :, 0:1]
 
     top, rest = pl.ds(0, half), pl.ds(half, half)
-    got(hid.at[DB, :, cols(1 - c, hidden)], h_r.at[DB])
-    for j in range(chips):
+    sides = ((0, XB, 0, 1, xn), (1, YB, 1, 0, yn))
+
+    def far_share(j):
         span = cols(fars[j], part)
         dsend[:, span] = low(down(DB, fars[j]))
         remote(dsend.at[top, span], din.at[0, :, span], d_s.at[0, j], d_r.at[0, j], xn)
         remote(dsend.at[rest, span], din.at[1, :, span], d_s.at[1, j], d_r.at[1, j], yn)
-    for i, block, now, later, dev in ((0, XB, 0, 1, xn), (1, YB, 1, 0, yn)):
-        got(hid.at[block, :, cols(1 - c, hidden)], h_r.at[block])
-        now_rows = slice(now * half, (now + 1) * half)
-        late_rows = slice(later * half, (later + 1) * half)
-        for j in range(chips):
-            span = cols(fars[j], part)
+
+    def early_share(j):
+        span = cols(fars[j], part)
+        for i, block, now, later, dev in sides:
             value = down(block, fars[j])
-            esend[i, :, span] = low(value[now_rows])
-            late[i, :, span] = value[late_rows]
-            remote(
-                esend.at[i, :, span],
-                xyin.at[i, pl.ds(now * half, half), span],
-                e_s.at[i, 0, j],
-                e_r.at[i, 0, j],
-                dev,
-            )
-    for j in range(chips):
+            esend[i, :, span] = low(value[now * half : (now + 1) * half])
+            late[i, :, span] = value[later * half : (later + 1) * half]
+            target = xyin.at[i, pl.ds(now * half, half), span]
+            remote(esend.at[i, :, span], target, e_s.at[i, 0, j], e_r.at[i, 0, j], dev)
+
+    def late_share(j):
         span = cols(fars[j], part)
-        for i, block, now, later, dev in ((0, XB, 0, 1, xn), (1, YB, 1, 0, yn)):
+        for i, block, now, later, dev in sides:
             got(din.at[1 - i, :, span], d_r.at[1 - i, j])
             lsend[i, :, span] = low(late[i, :, span] + f32(din[1 - i, :, span]))
-            remote(
-                lsend.at[i, :, span],
-                xyin.at[i, pl.ds(later * half, half), span],
-                e_s.at[i, 1, j],
-                e_r.at[i, 1, j],
-                dev,
-            )
-
-    @pl.when(jnp.logical_not(edge))
-    def _():
-        for j in range(chips - 1):
-            mixer_send(j)
-
-    z_finish(0, macc[:, cols(z, part)])
-
-    for j in range(chips):
-        p = fars[j]
-        span = cols(p, part)
-        for i, now, later in ((0, 0, 1), (1, 1, 0)):
+            target = xyin.at[i, pl.ds(later * half, half), span]
+            remote(lsend.at[i, :, span], target, e_s.at[i, 1, j], e_r.at[i, 1, j], dev)
+
+    def total_share(j):
+        span = cols(fars[j], part)
+        for i, block, now, later, dev in sides:
             got(xyin.at[i, pl.ds(now * half, half), span], e_r.at[i, 0, j])
             got(xyin.at[i, pl.ds(later * half, half), span], e_r.at[i, 1, j])
 
@@ -782,28 +801,57 @@
             return oacc[:, span] + f32(xyin[0, :, span]) + f32(xyin[1, :, span])
 
         if j < chips - 1:
-            z_send(1, j, p, total)
+            z_send(1, j, fars[j], total)
         else:
             z_finish(1, total())
 
+    got(hid.at[DB, :, cols(1 - c, hidden)], h_r.at[DB])
+    far_share(0)
+    got(hid.at[XB, :, cols(1 - c, hidden)], h_r.at[XB])
+    got(hid.at[YB, :, cols(1 - c, hidden)], h_r.at[YB])
+    early_share(0)
+    far_share(1)
+    at_middle(lambda: mixer_send(0))
+    late_share(0)
+    early_share(1)
+    far_share(2)
+    at_middle(lambda: mixer_send(1))
+    late_share(1)
+    early_share(2)
+    far_share(3)
+    at_middle(lambda: mixer_send(2))
+    total_share(0)
+    late_share(2)
+    early_share(3)
+    total_share(1)
+    late_share(3)
+    z_finish(0, macc[:, cols(z, part)])
+    total_share(2)
+    total_share(3)
+
     for kind, block in ((0, OWN), (1, DB)):
         for s in range(chips):
 
             @pl.when(has_r & (s <= z))
             def _():
-                sent(piece(block, s, c), ag_s.at[kind, 0, s])
+                for h in range(2):
+                    sent(halved(block, s, h), ag_s.at[kind, 0, s, h])
 
             @pl.when(has_l & (s >= z))
             def _():
-                sent(piece(block, s, c), ag_s.at[kind, 1, s])
-
+                for h in range(2):
+                    sent(halved(block, s, h), ag_s.at[kind, 1, s, h])
+
+    for i in range(2):
+        sent(halved(OWN, z, 0), xy_s.at[i, z])
+        sent(halved(OWN, z, 0), xy_s.at[i, chips])
+        for j in range(chips - 1):
+            sent(piece(OWN, nears[j], c), xy_s.at[i, nears[j]])
     for s in range(chips):
-        for i in range(2):
-            sent(piece(OWN, s, c), xy_s.at[i, s])
         for block in range(4):
             sent(piece(block, s, c), pt_s.at[block, s])
     for i in range(2):
-        sent(far_half(z, i), dr_s.at[i])
+        sent(halved(DB, z, i), dr_s.at[i])
         sent(kv_rows(OWN, 0, rows), kv_s.at[i])
         sent(kv_rows(OWN, 0, half), kv_s.at[2 + i])
     for i in range(3):
@@ -908,10 +956,10 @@
             dma((5 + 3 * chips,)),
             dma((3, chips)),
             dma((3, chips)),
-            dma((2, 2, chips)),
-            dma((2, chips)),
-            dma((2, chips)),
-            dma((2, chips)),
+            dma((2, 2, chips, 2)),
+            dma((2, chips, 2)),
+            dma((2, chips + 1)),
+            dma((2, chips + 1)),
             dma((2,)),
             dma((2,)),
             dma((4, chips)),
@@ -940,8 +988,8 @@
         diff_lambda,
         sub_gain[None, :],
         routed_input,
-        routes,
-        route_weights,
+        routes.T,
+        route_weights.T,
         table,
         out_weight,
         gate,

time: 128 us -> 102 us (0.80)
  Pallas kernels: 120 us -> 97.4 us
  local copies, waits for them, and re-layouts: 6.29 us -> 3.34 us
    pallas_call x1, Pallas kernels: 120 us -> 97.4 us  [kernel_body(): pl.pallas_call(functools.partial(layer_kernel, chips), out_shape=(out, ou...]
    unnamed x4 -> x2, local copies, waits for them, and re-layouts: 6.29 us -> 3.34 us
where the time goes in v1:
time: 102 us; the launch traced here: 101 us
  Pallas kernels  97.4 us (95%)
  local copies, waits for them, and re-layouts  3.34 us (3%)
    pallas_call x1, Pallas kernels, kernel_body(): pl.pallas_call(functools.partial(layer_kernel, chips), out_shape=(out, ou...  97.4 us
    unnamed x2, local copies, waits for them, and re-layouts  3.34 us

profile of v1, /device:TPU:0, one launch (start us, length us, event | category | flops | bytes accessed | tf_op | source)
XLA Modules:
  0.0 101.4 jit_solution(4544193280957714436)
XLA Ops:
  0.6 97.4 %layer.1 = (bf16[256,512]{1,0:T(8,128)(2,1)}, bf16[256,512]{1,0:T(8,128)(2,1)}) custom-call(bf16[256,256]{1,0:T(8,128)(2,1)} %q_ref.1, bf16[256,256]{1,0:T(8,128)(2,1)} %k_ref.1, bf16[256,256]{1,0:T(8,128)(2,1)} %v_ref.1, f32[2]{0:T(128)} %lam_ref.1, f32[1,128]{1,0:T(1,128)} %bitcast.11, bf16[256,512]{1,0:T(8,128)(2,1)} %x_ref.1, s32[2,256]{1,0:T(2,128)} %bitcast.9, ...), custom_call_target="tpu_custom_call" | custom-call | tf_op jit(solution)/shard_map/layer/pallas_call | solution.py:919
  98.0 1.7 %copy.20 = bf16[256,512]{1,0:T(8,128)(2,1)} copy(bf16[256,512]{1,0:T(8,128)(2,1)} %get-tuple-element.4) | data formatting | bytes 524288
  99.7 1.7 %copy.21 = bf16[256,512]{1,0:T(8,128)(2,1)} copy(bf16[256,512]{1,0:T(8,128)(2,1)} %get-tuple-element.5) | data formatting | bytes 524288

commit v2 on v1

--- a/solution.py
+++ b/solution.py
@@ -322,8 +322,10 @@
     qrot,
     sc_s,
     sc_p,
+    sc_m,
     sc_t,
     sc_o,
+    sc_a,
     ho,
     shtab,
     shcol,
@@ -391,6 +393,18 @@
     def cols(index, width):
         return pl.ds(pl.multiple_of(index * width, width), width)
 
+    barrier = pltpu.get_barrier_semaphore()
+    for dev in (pt, xn, yn):
+        pl.semaphore_signal(barrier, inc=1, device_id=dev, device_id_type=MESH)
+
+    @pl.when(has_r)
+    def _():
+        pl.semaphore_signal(barrier, inc=1, device_id=zr, device_id_type=MESH)
+
+    @pl.when(has_l)
+    def _():
+        pl.semaphore_signal(barrier, inc=1, device_id=zl, device_id_type=MESH)
+
     loads = [
         pltpu.make_async_copy(gw_hbm, guw.at[:, pl.ds(0, hidden)], w_l.at[0]),
         pltpu.make_async_copy(uw_hbm, guw.at[:, pl.ds(hidden, hidden)], w_l.at[1]),
@@ -412,25 +426,12 @@
     for i in list(range(4)) + list(range(5, len(loads))):
         loads[i].start()
 
-    barrier = pltpu.get_barrier_semaphore()
-    for dev in (pt, xn, yn):
-        pl.semaphore_signal(barrier, inc=1, device_id=dev, device_id_type=MESH)
-
-    @pl.when(has_r)
-    def _():
-        pl.semaphore_signal(barrier, inc=1, device_id=zr, device_id_type=MESH)
-
-    @pl.when(has_l)
-    def _():
-        pl.semaphore_signal(barrier, inc=1, device_id=zl, device_id_type=MESH)
-
-    pl.semaphore_wait(barrier, 3 + has_r.astype(jnp.int32) + has_l.astype(jnp.int32))
 
     def piece(block, s, core):
-        return xall.at[block, :, cols(2 * s + core, part)]
+        return xall.at[pl.ds(block * rows, rows), cols(2 * s + core, part)]
 
     def halved(block, s, h):
-        return xall.at[block, pl.ds(h * half, half), cols(2 * s + c, part)]
+        return xall.at[pl.ds(block * rows + h * half, half), cols(2 * s + c, part)]
 
     def z_forward(src, kind, block, s, h, right, left):
         @pl.when(right)
@@ -453,23 +454,6 @@
         block, dev = ((XB, xn), (YB, yn))[i]
         slot = z if order == 0 else chips
         remote(x_ref.at[pl.ds(h * half, half), :], halved(block, z, h), xy_s.at[i, slot], xy_r.at[i, slot], dev)
-
-    for h in range(2):
-        z_forward(x_ref.at[pl.ds(h * half, half), :], 0, OWN, z, h, has_r, has_l)
-    own_half(0, 0)
-    own_half(1, 0)
-    to_pair(x_ref, OWN, z)
-    xall[OWN, :, cols(t, part)] = x_ref[...]
-
-    expert_id = lax.broadcasted_iota(jnp.int32, (8, rows), 0)
-    routes = routes_ref[...]
-    weights = rw_ref[...]
-    table = jnp.zeros((8, rows), F32)
-    for k in range(routes.shape[0]):
-        table = table + jnp.where(routes[k : k + 1, :] == expert_id, weights[k : k + 1, :], 0.0)
-    shtab[OWN] = table
-    remote(shtab.at[OWN], shtab.at[XB], sh_s.at[0], sh_r.at[0], xn)
-    remote(shtab.at[OWN], shtab.at[YB], sh_s.at[1], sh_r.at[1], yn)
 
     loads[4].wait()
     cosine, sine = tab[:, :128], tab[:, 128:]
@@ -485,8 +469,30 @@
             if dst is None:
                 kv[0:rows, span] = turned
             else:
-                dst[:, span] = turned
+                turned = turned * jnp.asarray(qk ** (-0.5), BF16)
+                for m in range(2):
+                    in_map = (lax.broadcasted_iota(jnp.int32, (rows, 128), 1) // qk) == m
+                    dst[2 * i + m] = jnp.where(in_map, turned, jnp.zeros((rows, 128), BF16))
     kv[0:rows, kwide:] = v_ref[...]
+
+    pl.semaphore_wait(barrier, 3 + has_r.astype(jnp.int32) + has_l.astype(jnp.int32))
+
+    for h in range(2):
+        z_forward(x_ref.at[pl.ds(h * half, half), :], 0, OWN, z, h, has_r, has_l)
+    own_half(0, 0)
+    own_half(1, 0)
+    to_pair(x_ref, OWN, z)
+    xall[0:rows, cols(t, part)] = x_ref[...]
+
+    expert_id = lax.broadcasted_iota(jnp.int32, (8, rows), 0)
+    routes = routes_ref[...]
+    weights = rw_ref[...]
+    table = jnp.zeros((8, rows), F32)
+    for k in range(routes.shape[0]):
+        table = table + jnp.where(routes[k : k + 1, :] == expert_id, weights[k : k + 1, :], 0.0)
+    shtab[OWN] = table
+    remote(shtab.at[OWN], shtab.at[XB], sh_s.at[0], sh_r.at[0], xn)
+    remote(shtab.at[OWN], shtab.at[YB], sh_s.at[1], sh_r.at[1], yn)
 
     def kv_rows(block, start, count):
         return kv.at[pl.ds(block * rows + start, count), :]
@@ -508,36 +514,46 @@
                 pt,
             )
 
-    def chunk(block, s, first, weight, target, width):
+    def chunk(block, count, at, depth, first, weight, target, base, width):
         tiles = target.shape[-1] // width
+        left_rows, target_rows = pl.ds(block * rows, count * rows), pl.ds(base * rows, count * rows)
 
         def tile(n, carry):
             span = cols(n, width)
-            value = mm(xall[block, :, cols(s, wide)], weight[cols(s, wide), span])
+            value = mm(xall[left_rows, cols(at, depth)], weight[cols(at, depth), span])
             if not first:
-                value = value + target[:, span]
-            target[:, span] = value
+                value = value + target[target_rows, span]
+            target[target_rows, span] = value
             return carry
 
         lax.fori_loop(0, tiles, tile, 0)
 
-    def squares(block, s, first):
-        total = jnp.zeros((rows, 128), F32) if first else ssq[block]
-        for i in range(wide // 128):
-            value = f32(xall[block, :, pl.ds(pl.multiple_of(s * wide + i * 128, 128), 128)])
+    def squares(block, count, at, depth, first):
+        span = pl.ds(block * rows, count * rows)
+        total = jnp.zeros((count * rows, 128), F32) if first else ssq[span, :]
+        for i in range(depth // 128):
+            value = f32(xall[span, pl.ds(pl.multiple_of(at * depth + i * 128, 128), 128)])
             total = total + value * value
-        ssq[block] = total
-
-    def expert_chunk(block, s, first):
-        got(piece(block, s, 1 - c), pt_r.at[block, s])
-        chunk(block, s, first, guw, acc.at[block], hidden)
-        squares(block, s, first)
+        ssq[span, :] = total
+
+    def expert_chunk(block, s, first, count=1):
+        for b in range(block, block + count):
+            got(piece(b, s, 1 - c), pt_r.at[b, s])
+        chunk(block, count, s, wide, first, guw, acc, block, hidden)
+        squares(block, count, s, wide, first)
+
+    def expert_half(block, s, core, count=1):
+        if core is not c:
+            for b in range(block, block + count):
+                got(piece(b, s, 1 - c), pt_r.at[b, s])
+        chunk(block, count, 2 * s + core, part, False, guw, acc, block, hidden)
+        squares(block, count, 2 * s + core, part, False)
 
     def shared_chunk(s, first):
-        chunk(OWN, s, first, sgu, sacc, 2 * shared)
+        chunk(OWN, 1, s, wide, first, sgu, sacc, 0, 2 * shared)
 
     def activate(block, source, width, target, index):
-        full = jnp.sum(ssq[block], axis=1, keepdims=True) / (chips * wide)
+        full = jnp.sum(ssq[pl.ds(block * rows, rows), :], axis=1, keepdims=True) / (chips * wide)
         factor = lax.rsqrt(full + NORM_EPS)
         gate = source[:, :width] * factor
         up = source[:, width:] * factor
@@ -574,15 +590,80 @@
             for j in orders:
                 z_arrival(kind, nears[j], h)
 
+    def value_cols(h):
+        return pl.ds(kwide + h * vd, vd)
+
+    step_rows = 64
+    ids = (e, xn[0], yn[0], xn[0] + yn[0] - e)
+    bias = [jnp.where(ids[b] < e, 0.0, MASKED) for b in range(4)]
+
+    def attend_first(i):
+        count = 3 * rows
+        sc_s[...] = lax.dot_general(
+            qrot[i], kv[0:count, cols(i // 2, 128)], (((1,), (1,)), ((), ())), preferred_element_type=F32
+        )
+
+        for r in range(0, rows, step_rows):
+            at = slice(r, r + step_rows)
+            key = lax.broadcasted_iota(jnp.int32, (step_rows, rows), 1)
+            row = r + lax.broadcasted_iota(jnp.int32, (step_rows, rows), 0)
+            scores = [
+                jnp.where(key <= row, sc_s[at, 0:rows], MASKED),
+                sc_s[at, rows : 2 * rows] + bias[XB],
+                sc_s[at, 2 * rows :] + bias[YB],
+            ]
+            most = jnp.maximum(jnp.maximum(scores[0], scores[1]), scores[2])
+            most = jnp.max(most, axis=1, keepdims=True)
+            weight = [jnp.exp(score - most) for score in scores]
+            total = jnp.sum(weight[0] + weight[1] + weight[2], axis=1, keepdims=True)
+            for b in range(3):
+                sc_p[at, b * rows : (b + 1) * rows] = low(weight[b])
+            sc_m[i, at, :] = jnp.broadcast_to(most, (step_rows, 128))
+            sc_t[i, at, :] = jnp.broadcast_to(total, (step_rows, 128))
+
+        sc_o[i] = mm(sc_p[...], kv[0:count, value_cols(i // 2)])
+
+    def attend_last(i):
+        count = 3 * rows
+        sc_s[:, 0:rows] = lax.dot_general(
+            qrot[i], kv[count:, cols(i // 2, 128)], (((1,), (1,)), ((), ())), preferred_element_type=F32
+        )
+
+        for r in range(0, rows, step_rows):
+            at = slice(r, r + step_rows)
+            scores = sc_s[at, 0:rows] + bias[DB]
+            before = sc_m[i, at, :]
+            most = jnp.maximum(before, jnp.max(scores, axis=1, keepdims=True))
+            weight = jnp.exp(scores - most[:, 0:1])
+            shrink = jnp.exp(before - most)
+            sc_p[at, 0:rows] = low(weight)
+            sc_a[at, :] = shrink
+            sc_t[i, at, :] = sc_t[i, at, :] * shrink + jnp.sum(weight, axis=1, keepdims=True)
+
+        return (sc_o[i] * sc_a[...] + mm(sc_p[:, 0:rows], kv[count:, value_cols(i // 2)])) / sc_t[i]
+
+    def finish_head(h):
+        sc_o[2 * h] = attend_last(2 * h)
+        mixed = sc_o[2 * h] - lam_ref[h] * attend_last(2 * h + 1)
+        scale = lax.rsqrt(jnp.mean(mixed * mixed, axis=1, keepdims=True) + NORM_EPS)
+        ho[:, pl.ds(pl.multiple_of(c * vwide + h * vd, 128), vd)] = low(mixed * scale * gain_ref[...])
+
+    loads[0].wait()
+    loads[1].wait()
+    expert_chunk(OWN, z, True)
+    at_middle(lambda: [z_arrival(0, nears[j], 0) for j in (0, 1)])
+    loads[2].wait()
+    loads[3].wait()
+    shared_chunk(z, True)
     got(halved(XB, z, 0), xy_r.at[0, z])
     got(halved(YB, z, 1), xy_r.at[1, z])
     remote(halved(XB, z, 0), halved(DB, z, 0), dr_s.at[0], dr_r.at[0], yn)
     remote(halved(YB, z, 1), halved(DB, z, 1), dr_s.at[1], dr_r.at[1], xn)
-    at_middle(lambda: arrivals(0, 0, 1))
+    at_middle(lambda: [z_arrival(0, nears[j], 1) for j in (0, 1)])
     at_edge(lambda: arrivals(0, 0))
-    loads[0].wait()
-    loads[1].wait()
-    expert_chunk(OWN, z, True)
+    at_middle(lambda: z_arrival(0, nears[2], 0))
+    expert_chunk(OWN, nears[0], False)
+    shared_chunk(nears[0], False)
     got(kv_rows(XB, 0, rows), kv_r.at[0])
     got(kv_rows(YB, 0, rows), kv_r.at[1])
     remote(kv_rows(XB, 0, half), kv_rows(DB, 0, half), kv_s.at[2], kv_r.at[2], yn)
@@ -592,24 +673,26 @@
     remote(shtab.at[XB], shtab.at[DB], sh_s.at[2], sh_r.at[2], yn)
     to_xy(nears[0])
     at_middle(lambda: to_xy(nears[1]))
+    at_middle(lambda: z_arrival(0, nears[2], 1))
+    at_middle(lambda: to_xy(nears[2]))
+    attend_first(0)
+    attend_first(1)
     got(halved(XB, z, 1), xy_r.at[0, chips])
     got(halved(YB, z, 0), xy_r.at[1, chips])
     to_pair(piece(XB, z, c), XB, z)
     to_pair(piece(YB, z, c), YB, z)
-    at_middle(lambda: arrivals(0, 2))
     at_edge(lambda: arrivals(0, 1))
-    at_middle(lambda: to_xy(nears[2]))
     at_edge(lambda: to_xy(nears[1]))
-    give_down(0)
-    expert_chunk(OWN, nears[0], False)
-    loads[2].wait()
-    loads[3].wait()
-    shared_chunk(z, True)
     got(halved(DB, z, 0), dr_r.at[0])
     got(halved(DB, z, 1), dr_r.at[1])
     for h in range(2):
         z_forward(halved(DB, z, h), 1, DB, z, h, has_r, has_l)
     to_pair(piece(DB, z, c), DB, z)
+    give_down(0)
+    attend_first(2)
+    attend_first(3)
+    expert_chunk(OWN, nears[1], False)
+    shared_chunk(nears[1], False)
 
     def last_own():
         arrivals(0, 2)
@@ -618,53 +701,22 @@
     at_edge(last_own)
     give_down(1)
     give_down(2)
-    expert_chunk(OWN, nears[1], False)
+    expert_chunk(XB, z, True, 2)
+    at_middle(lambda: [z_arrival(1, nears[j], 0) for j in (0, 1)])
     got(kv_rows(DB, 0, half), kv_r.at[2])
     got(kv_rows(DB, half, half), kv_r.at[3])
-    key_count = kv.shape[0]
-    step_rows = 32
-    ids = (e, xn[0], yn[0], xn[0] + yn[0] - e)
-
-    def one_map(h, m):
-        in_map = (lax.broadcasted_iota(jnp.int32, (rows, 128), 1) // qk) == m
-        query = jnp.where(in_map, qrot[:, cols(h, 128)], jnp.zeros((rows, 128), BF16))
-        sc_s[...] = lax.dot_general(
-            query, kv[:, cols(h, 128)], (((1,), (1,)), ((), ())), preferred_element_type=F32
-        )
-
-        def soften(r, carry):
-            at = pl.ds(pl.multiple_of(r * step_rows, step_rows), step_rows)
-            key = lax.broadcasted_iota(jnp.int32, (step_rows, key_count), 1)
-            which = key // rows
-            group = jnp.where(
-                which == 0, ids[0], jnp.where(which == 1, ids[1], jnp.where(which == 2, ids[2], ids[3]))
-            )
-            key_at = group * rows + key % rows
-            query_at = (
-                e * rows + r * step_rows + lax.broadcasted_iota(jnp.int32, (step_rows, key_count), 0)
-            )
-            scores = jnp.where(key_at <= query_at, sc_s[at, :] * (qk ** (-0.5)), MASKED)
-            weight = jnp.exp(scores - jnp.max(scores, axis=1, keepdims=True))
-            total = jnp.sum(weight, axis=1, keepdims=True)
-            sc_p[at, :] = low(weight)
-            sc_t[at, :] = jnp.broadcast_to(total, (step_rows, 128))
-            return carry
-
-        lax.fori_loop(0, rows // step_rows, soften, 0)
-        return mm(sc_p[...], kv[:, pl.ds(pl.multiple_of(kwide + h * vd, 128), vd)]) / sc_t[...]
-
-    for h in range(local_heads):
-        sc_o[...] = one_map(h, 0)
-        at_middle(lambda: [z_arrival(1, nears[j], h) for j in (0, 1)])
-        mixed = sc_o[...] - lam_ref[h] * one_map(h, 1)
-        scale = lax.rsqrt(jnp.mean(mixed * mixed, axis=1, keepdims=True) + NORM_EPS)
-        ho[:, pl.ds(pl.multiple_of(c * vwide + h * vd, 128), vd)] = low(mixed * scale * gain_ref[...])
+    finish_head(0)
+    finish_head(1)
     mine = ho.at[:, cols(c, vwide)]
     remote(mine, mine, h_s.at[5], h_r.at[5], pt)
+    at_middle(lambda: [z_arrival(1, nears[j], 1) for j in (0, 1)])
+    expert_chunk(DB, z, True)
+    expert_chunk(OWN, nears[2], False)
+    activate(OWN, acc.at[pl.ds(OWN * rows, rows), :], hidden, hid.at[OWN], OWN)
+    shared_chunk(nears[2], False)
+    activate(OWN, sacc, shared, shid, 4)
     at_edge(lambda: arrivals(1, 0))
     side_arrival(nears[0])
-    expert_chunk(XB, z, True)
-    expert_chunk(YB, z, True)
     for p in range(chips):
         loads[5 + p].wait()
         got(ow.at[cols(1 - c, vwide), pl.ds(p * part, part)], w_r.at[0, p])
@@ -672,6 +724,7 @@
     for j in range(chips):
         span = cols(fars[j], part)
         macc[:, span] = mm(ho[...], ow[:, span])
+
     def z_send(kind, j, p, value_of):
         upstream = ((p > z) & has_l) | ((p < z) & has_r)
         slot = zout.at[kind, j]
@@ -725,17 +778,7 @@
         z_send(0, j, p, lambda: macc[:, cols(p, part)])
 
     at_edge(lambda: [mixer_send(j) for j in range(chips - 1)])
-    at_middle(lambda: arrivals(1, 2))
-    expert_chunk(DB, z, True)
-    expert_chunk(OWN, nears[2], False)
-    activate(OWN, acc.at[OWN], hidden, hid.at[OWN], OWN)
-    for j in range(chips - 1):
-        shared_chunk(nears[j], False)
-    activate(OWN, sacc, shared, shid, 4)
-    for block in (XB, YB, DB):
-        expert_chunk(block, nears[0], False)
-    at_edge(lambda: arrivals(1, 1))
-    side_arrival(nears[1])
+    at_middle(lambda: z_arrival(1, nears[2], 0))
     for p in range(chips):
         loads[5 + chips + p].wait()
         loads[5 + 2 * chips + p].wait()
@@ -753,14 +796,19 @@
         oacc[:, span] = mm(hid[OWN], dw[:, span]) * shcol[OWN, :, 0:1] + mm(shid[...], sd[:, span])
         return carry
 
-    for block in (XB, YB, DB):
-        expert_chunk(block, nears[1], False)
     lax.fori_loop(0, chips, own_down, 0)
+    at_middle(lambda: z_arrival(1, nears[2], 1))
+    at_edge(lambda: arrivals(1, 1))
+    side_arrival(nears[1])
+    expert_chunk(XB, nears[0], False, 3)
+    expert_chunk(XB, nears[1], False, 3)
     at_edge(lambda: arrivals(1, 2))
     side_arrival(nears[2])
-    for block in (DB, XB, YB):
-        expert_chunk(block, nears[2], False)
-        activate(block, acc.at[block], hidden, hid.at[block], block)
+    expert_half(DB, nears[2], c)
+    expert_half(XB, nears[2], c, 2)
+    expert_half(DB, nears[2], 1 - c)
+    activate(DB, acc.at[pl.ds(DB * rows, rows), :], hidden, hid.at[DB], DB)
+    expert_half(XB, nears[2], 1 - c, 2)
 
     def down(block, p):
         return mm(hid[block], dw[:, cols(p, part)]) * shcol[block, :, 0:1]
@@ -807,6 +855,8 @@
 
     got(hid.at[DB, :, cols(1 - c, hidden)], h_r.at[DB])
     far_share(0)
+    activate(XB, acc.at[pl.ds(XB * rows, rows), :], hidden, hid.at[XB], XB)
+    activate(YB, acc.at[pl.ds(YB * rows, rows), :], hidden, hid.at[YB], YB)
     got(hid.at[XB, :, cols(1 - c, hidden)], h_r.at[XB])
     got(hid.at[YB, :, cols(1 - c, hidden)], h_r.at[YB])
     early_share(0)
@@ -870,6 +920,15 @@
             sent(lsend.at[i, :, pl.ds(j * part, part)], e_s.at[i, 1, j])
         for j in range(chips - 1):
             sent(zout.at[i, j], z_s.at[i, j])
+
+
+def emit_kernel(mixed_ref, routed_ref, mix_hbm, out_hbm, sems):
+    first = pltpu.make_async_copy(mixed_ref, mix_hbm, sems.at[0])
+    second = pltpu.make_async_copy(routed_ref, out_hbm, sems.at[1])
+    first.start()
+    second.start()
+    first.wait()
+    second.wait()
 
 
 def rotation_table(positions, key_width):
@@ -916,22 +975,22 @@
     hbm = pl.BlockSpec(memory_space=pl.ANY)
     dma = pltpu.SemaphoreType.DMA
     out = jax.ShapeDtypeStruct((rows, part), BF16)
-    return pl.pallas_call(
+    mixed, routed = pl.pallas_call(
         functools.partial(layer_kernel, chips),
         out_shape=(out, out),
         in_specs=[vmem, vmem, vmem, smem, vmem, vmem, vmem, vmem] + [hbm] * 8,
         out_specs=(vmem, vmem),
         scratch_shapes=[
-            pltpu.VMEM((groups, rows, width), BF16),
+            pltpu.VMEM((groups * rows, width), BF16),
             pltpu.VMEM((width, 2 * hidden), BF16),
             pltpu.VMEM((2 * hidden, mine), BF16),
             pltpu.VMEM((width, 2 * shared), BF16),
             pltpu.VMEM((2 * shared, mine), BF16),
             pltpu.VMEM((2 * vwide, mine), BF16),
             pltpu.VMEM((rows, 256), F32),
-            pltpu.VMEM((groups, rows, 2 * hidden), F32),
+            pltpu.VMEM((groups * rows, 2 * hidden), F32),
             pltpu.VMEM((rows, 2 * shared), F32),
-            pltpu.VMEM((groups, rows, 128), F32),
+            pltpu.VMEM((groups * rows, 128), F32),
             pltpu.VMEM((groups, rows, 2 * hidden), BF16),
             pltpu.VMEM((rows, 2 * shared), BF16),
             pltpu.VMEM((rows, mine), F32),
@@ -945,10 +1004,12 @@
             pltpu.VMEM((2, chips - 1, rows, part), BF16),
             pltpu.VMEM((rows, mine), F32),
             pltpu.VMEM((groups * rows, kwide + vwide), BF16),
-            pltpu.VMEM((rows, kwide), BF16),
-            pltpu.VMEM((rows, groups * rows), F32),
-            pltpu.VMEM((rows, groups * rows), BF16),
-            pltpu.VMEM((rows, 128), F32),
+            pltpu.VMEM((2 * local_heads, rows, 128), BF16),
+            pltpu.VMEM((rows, 3 * rows), F32),
+            pltpu.VMEM((rows, 3 * rows), BF16),
+            pltpu.VMEM((2 * local_heads, rows, 128), F32),
+            pltpu.VMEM((2 * local_heads, rows, 128), F32),
+            pltpu.VMEM((2 * local_heads, rows, 128), F32),
             pltpu.VMEM((rows, 128), F32),
             pltpu.VMEM((rows, 2 * vwide), BF16),
             pltpu.VMEM((groups, 8, rows), F32),
@@ -999,6 +1060,14 @@
         shared_up,
         shared_down,
     )
+    return pl.pallas_call(
+        emit_kernel,
+        out_shape=(out, out),
+        in_specs=[vmem, vmem],
+        out_specs=(hbm, hbm),
+        scratch_shapes=[dma((2,))],
+        name="emit",
+    )(mixed, routed)
 
 
 def solution(mesh):

time: 102 us -> 88.4 us (0.87)
  Pallas kernels: 97.4 us -> 86.6 us
  local copies, waits for them, and re-layouts: 3.34 us -> 0 us
    pallas_call x1, Pallas kernels: 97.4 us -> 84.8 us  [kernel_body(): pl.pallas_call(functools.partial(layer_kernel, chips), out_shape=(out, ou...]
    unnamed x2 -> x0, local copies, waits for them, and re-layouts: 3.34 us -> none
    pallas_call x0 -> x1, Pallas kernels: none -> 1.83 us  [kernel_body(): pl.pallas_call(emit_kernel, out_shape=(out, out), in_specs=[vmem, vmem],...]
where the time goes in v2:
time: 88.4 us; the launch traced here: 87.4 us
  Pallas kernels  86.6 us (98%)
    pallas_call x1, Pallas kernels, kernel_body(): pl.pallas_call(functools.partial(layer_kernel, chips), out_shape=(out, ou...  84.8 us
    pallas_call x1, Pallas kernels, kernel_body(): pl.pallas_call(emit_kernel, out_shape=(out, out), in_specs=[vmem, vmem],...  1.83 us

profile of v2, /device:TPU:0, one launch (start us, length us, event | category | flops | bytes accessed | tf_op | source)
XLA Modules:
  0.0 87.4 jit_solution(14320570692204576018)
XLA Ops:
  0.6 84.8 %layer.1 = (bf16[256,512]{1,0:T(8,128)(2,1)}, bf16[256,512]{1,0:T(8,128)(2,1)}) custom-call(bf16[256,256]{1,0:T(8,128)(2,1)} %q_ref.1, bf16[256,256]{1,0:T(8,128)(2,1)} %k_ref.1, bf16[256,256]{1,0:T(8,128)(2,1)} %v_ref.1, f32[2]{0:T(128)} %lam_ref.1, f32[1,128]{1,0:T(1,128)} %bitcast.11, bf16[256,512]{1,0:T(8,128)(2,1)} %x_ref.1, s32[2,256]{1,0:T(2,128)} %bitcast.9, ...), custom_call_target="tpu_custom_call" | custom-call | tf_op jit(solution)/shard_map/layer/pallas_call | solution.py:978
  85.4 1.8 %emit.1 = (bf16[256,512]{1,0:T(8,128)(2,1)}, bf16[256,512]{1,0:T(8,128)(2,1)}) custom-call(bf16[256,512]{1,0:T(8,128)(2,1)} %get-tuple-element.4.mixed_ref, bf16[256,512]{1,0:T(8,128)(2,1)} %get-tuple-element.5.routed_ref), custom_call_target="tpu_custom_call" | custom-call | tf_op jit(solution)/shard_map/emit/pallas_call | solution.py:1063

commit v3 on v2

--- a/solution.py
+++ b/solution.py
@@ -278,14 +278,14 @@
 
 def layer_kernel(
     chips,
-    q_ref,
-    k_ref,
-    v_ref,
     lam_ref,
-    gain_ref,
-    x_ref,
-    routes_ref,
-    rw_ref,
+    q_hbm,
+    k_hbm,
+    v_hbm,
+    gain_hbm,
+    x_hbm,
+    routes_hbm,
+    rw_hbm,
     tab_hbm,
     ow_hbm,
     gw_hbm,
@@ -294,6 +294,8 @@
     sg_hbm,
     su_hbm,
     sd_hbm,
+    mix_hbm,
+    out_hbm,
     mix_ref,
     out_ref,
     xall,
@@ -303,6 +305,11 @@
     sd,
     ow,
     tab,
+    q_ref,
+    k_ref,
+    gain_ref,
+    routes_ref,
+    rw_ref,
     acc,
     sacc,
     ssq,
@@ -352,14 +359,15 @@
     e_r,
     z_s,
     z_r,
+    in_l,
 ):
-    rows, part = x_ref.shape
+    rows, part = x_hbm.shape
     half = rows // 2
     wide = 2 * part
     hidden = gw_hbm.shape[1]
     shared = sg_hbm.shape[1]
-    vwide = v_ref.shape[1]
-    kwide = k_ref.shape[1]
+    vwide = v_hbm.shape[1]
+    kwide = k_hbm.shape[1]
     local_heads = lam_ref.shape[0]
     vd = vwide // local_heads
     qk = kwide // (2 * local_heads)
@@ -422,16 +430,32 @@
                     w_l.at[5 + i * chips + p],
                 )
             )
+    own_rows = pl.ds(0, rows)
+    inputs = [
+        pltpu.make_async_copy(x_hbm, xall.at[own_rows, cols(t, part)], in_l.at[0]),
+        pltpu.make_async_copy(q_hbm, q_ref, in_l.at[1]),
+        pltpu.make_async_copy(k_hbm, k_ref, in_l.at[2]),
+        pltpu.make_async_copy(v_hbm, kv.at[own_rows, pl.ds(kwide, vwide)], in_l.at[3]),
+        pltpu.make_async_copy(routes_hbm, routes_ref, in_l.at[4]),
+        pltpu.make_async_copy(rw_hbm, rw_ref, in_l.at[5]),
+        pltpu.make_async_copy(gain_hbm, gain_ref, in_l.at[6]),
+    ]
+    inputs[0].start()
+    inputs[1].start()
+    inputs[2].start()
     loads[4].start()
-    for i in list(range(4)) + list(range(5, len(loads))):
-        loads[i].start()
+    for copy in inputs[3:]:
+        copy.start()
 
 
     def piece(block, s, core):
         return xall.at[pl.ds(block * rows, rows), cols(2 * s + core, part)]
 
-    def halved(block, s, h):
-        return xall.at[pl.ds(block * rows + h * half, half), cols(2 * s + c, part)]
+    def base(block, h):
+        return block * rows + (h if block in (OWN, DB) else 1 - h) * half
+
+    def halved(block, s, h, core=None):
+        return xall.at[pl.ds(base(block, h), half), cols(2 * s + (c if core is None else core), part)]
 
     def z_forward(src, kind, block, s, h, right, left):
         @pl.when(right)
@@ -443,18 +467,64 @@
             remote(src, halved(block, s, h), ag_s.at[kind, 1, s, h], ag_r.at[kind, s, h], zl)
 
     def to_pair(src, block, s):
-        remote(src, piece(block, s, c), pt_s.at[block, s], pt_r.at[block, s], pt)
+        remote(src, piece(block, s, c), pt_s.at[block, s, 0], pt_r.at[block, s, 0], pt)
+
+    def half_of(i, order):
+        return order if i == 0 else 1 - order
+
+    def to_side(i, order, s, src):
+        block, dev = ((XB, xn), (YB, yn))[i]
+        target = halved(block, s, half_of(i, order))
+        remote(src, target, xy_s.at[i, s, order], xy_r.at[i, s, order], dev)
+
+    def own_half(i, order):
+        to_side(i, order, z, halved(OWN, z, half_of(i, order)))
 
     def to_xy(s):
-        remote(piece(OWN, s, c), piece(XB, s, c), xy_s.at[0, s], xy_r.at[0, s], xn)
-        remote(piece(OWN, s, c), piece(YB, s, c), xy_s.at[1, s], xy_r.at[1, s], yn)
-
-    def own_half(i, order):
-        h = order if i == 0 else 1 - order
-        block, dev = ((XB, xn), (YB, yn))[i]
-        slot = z if order == 0 else chips
-        remote(x_ref.at[pl.ds(h * half, half), :], halved(block, z, h), xy_s.at[i, slot], xy_r.at[i, slot], dev)
-
+        for order in range(2):
+            for i in range(2):
+                to_side(i, order, s, halved(OWN, s, half_of(i, order)))
+
+    def side_half(i, order, s, core=None):
+        return halved((XB, YB)[i], s, half_of(i, order), core)
+
+    def side_arrival(s, order):
+        for i, block in ((0, XB), (1, YB)):
+            mine = side_half(i, order, s)
+            got(mine, xy_r.at[i, s, order])
+            remote(mine, mine, pt_s.at[block, s, order], pt_r.at[block, s, order], pt)
+
+    def paired(block, s):
+        got(piece(block, s, 1 - c), pt_r.at[block, s, 0])
+
+    def paired_half(i, order, s):
+        got(side_half(i, order, s, 1 - c), pt_r.at[(XB, YB)[i], s, order])
+
+    inputs[0].wait()
+    loads[0].start()
+    loads[1].start()
+    pl.semaphore_wait(barrier, 3 + has_r.astype(jnp.int32) + has_l.astype(jnp.int32))
+
+    for h in range(2):
+        z_forward(halved(OWN, z, h), 0, OWN, z, h, has_r, has_l)
+    own_half(0, 0)
+    own_half(1, 0)
+    to_pair(piece(OWN, z, c), OWN, z)
+
+    expert_id = lax.broadcasted_iota(jnp.int32, (8, rows), 0)
+    inputs[4].wait()
+    inputs[5].wait()
+    routes = routes_ref[...]
+    weights = rw_ref[...]
+    table = jnp.zeros((8, rows), F32)
+    for k in range(routes.shape[0]):
+        table = table + jnp.where(routes[k : k + 1, :] == expert_id, weights[k : k + 1, :], 0.0)
+    shtab[OWN] = table
+    remote(shtab.at[OWN], shtab.at[XB], sh_s.at[0], sh_r.at[0], xn)
+    remote(shtab.at[OWN], shtab.at[YB], sh_s.at[1], sh_r.at[1], yn)
+
+    for copy in inputs[1:4]:
+        copy.wait()
     loads[4].wait()
     cosine, sine = tab[:, :128], tab[:, 128:]
     at_row = lax.broadcasted_iota(jnp.int32, (128, 128), 0)
@@ -473,26 +543,6 @@
                 for m in range(2):
                     in_map = (lax.broadcasted_iota(jnp.int32, (rows, 128), 1) // qk) == m
                     dst[2 * i + m] = jnp.where(in_map, turned, jnp.zeros((rows, 128), BF16))
-    kv[0:rows, kwide:] = v_ref[...]
-
-    pl.semaphore_wait(barrier, 3 + has_r.astype(jnp.int32) + has_l.astype(jnp.int32))
-
-    for h in range(2):
-        z_forward(x_ref.at[pl.ds(h * half, half), :], 0, OWN, z, h, has_r, has_l)
-    own_half(0, 0)
-    own_half(1, 0)
-    to_pair(x_ref, OWN, z)
-    xall[0:rows, cols(t, part)] = x_ref[...]
-
-    expert_id = lax.broadcasted_iota(jnp.int32, (8, rows), 0)
-    routes = routes_ref[...]
-    weights = rw_ref[...]
-    table = jnp.zeros((8, rows), F32)
-    for k in range(routes.shape[0]):
-        table = table + jnp.where(routes[k : k + 1, :] == expert_id, weights[k : k + 1, :], 0.0)
-    shtab[OWN] = table
-    remote(shtab.at[OWN], shtab.at[XB], sh_s.at[0], sh_r.at[0], xn)
-    remote(shtab.at[OWN], shtab.at[YB], sh_s.at[1], sh_r.at[1], yn)
 
     def kv_rows(block, start, count):
         return kv.at[pl.ds(block * rows + start, count), :]
@@ -502,6 +552,8 @@
 
     own_half(0, 1)
     own_half(1, 1)
+    for i in list(range(2, 4)) + list(range(5, len(loads))):
+        loads[i].start()
 
     def give_down(i):
         src, dst, depth = downs[i]
@@ -514,52 +566,59 @@
                 pt,
             )
 
-    def chunk(block, count, at, depth, first, weight, target, base, width):
+    def chunk(start, count, at, depth, first, weight, target, width):
         tiles = target.shape[-1] // width
-        left_rows, target_rows = pl.ds(block * rows, count * rows), pl.ds(base * rows, count * rows)
+        span_rows = pl.ds(start, count)
 
         def tile(n, carry):
             span = cols(n, width)
-            value = mm(xall[left_rows, cols(at, depth)], weight[cols(at, depth), span])
+            value = mm(xall[span_rows, cols(at, depth)], weight[cols(at, depth), span])
             if not first:
-                value = value + target[target_rows, span]
-            target[target_rows, span] = value
+                value = value + target[span_rows, span]
+            target[span_rows, span] = value
             return carry
 
         lax.fori_loop(0, tiles, tile, 0)
 
-    def squares(block, count, at, depth, first):
-        span = pl.ds(block * rows, count * rows)
-        total = jnp.zeros((count * rows, 128), F32) if first else ssq[span, :]
+    def squares(start, count, at, depth, first):
+        span = pl.ds(start, count)
+        total = jnp.zeros((count, 128), F32) if first else ssq[span, :]
         for i in range(depth // 128):
             value = f32(xall[span, pl.ds(pl.multiple_of(at * depth + i * 128, 128), 128)])
             total = total + value * value
         ssq[span, :] = total
 
+    def expert_rows(start, count, at, depth, first=False):
+        chunk(start, count, at, depth, first, guw, acc, hidden)
+        squares(start, count, at, depth, first)
+
     def expert_chunk(block, s, first, count=1):
         for b in range(block, block + count):
-            got(piece(b, s, 1 - c), pt_r.at[b, s])
-        chunk(block, count, s, wide, first, guw, acc, block, hidden)
-        squares(block, count, s, wide, first)
-
-    def expert_half(block, s, core, count=1):
-        if core is not c:
-            for b in range(block, block + count):
-                got(piece(b, s, 1 - c), pt_r.at[b, s])
-        chunk(block, count, 2 * s + core, part, False, guw, acc, block, hidden)
-        squares(block, count, 2 * s + core, part, False)
+            if b in (OWN, DB):
+                paired(b, s)
+            else:
+                for order in range(2):
+                    paired_half(b - XB, order, s)
+        expert_rows(block * rows, count * rows, s, wide, first)
 
     def shared_chunk(s, first):
-        chunk(OWN, 1, s, wide, first, sgu, sacc, 0, 2 * shared)
-
-    def activate(block, source, width, target, index):
-        full = jnp.sum(ssq[pl.ds(block * rows, rows), :], axis=1, keepdims=True) / (chips * wide)
+        chunk(0, rows, s, wide, first, sgu, sacc, 2 * shared)
+
+    def activate(start, count, source, width, target, target_start, index):
+        full = jnp.sum(ssq[pl.ds(start, count), :], axis=1, keepdims=True) / (chips * wide)
         factor = lax.rsqrt(full + NORM_EPS)
-        gate = source[:, :width] * factor
-        up = source[:, width:] * factor
-        target[:, cols(c, width)] = low(gate / (1.0 + jnp.exp(-gate)) * up)
-        mine = target.at[:, cols(c, width)]
+        span = pl.ds(target_start, count)
+        gate = source[span, :width] * factor
+        up = source[span, width:] * factor
+        target[span, cols(c, width)] = low(gate / (1.0 + jnp.exp(-gate)) * up)
+        mine = target.at[span, cols(c, width)]
         remote(mine, mine, h_s.at[index], h_r.at[index], pt)
+
+    def expert_activate(start, count, index):
+        activate(start, count, acc, hidden, hid, start, index)
+
+    def expert_hidden(start, count, index):
+        got(hid.at[pl.ds(start, count), cols(1 - c, hidden)], h_r.at[index])
 
     def z_arrival(kind, s, h):
         block = (OWN, DB)[kind]
@@ -568,11 +627,6 @@
         if h == 1:
             to_pair(piece(block, s, c), block, s)
 
-    def side_arrival(s):
-        for i, block in ((0, XB), (1, YB)):
-            got(piece(block, s, c), xy_r.at[i, s])
-            to_pair(piece(block, s, c), block, s)
-
     middle = has_l & has_r
 
     def at_middle(work):
@@ -596,6 +650,8 @@
     step_rows = 64
     ids = (e, xn[0], yn[0], xn[0] + yn[0] - e)
     bias = [jnp.where(ids[b] < e, 0.0, MASKED) for b in range(4)]
+
+    inputs[6].wait()
 
     def attend_first(i):
         count = 3 * rows
@@ -655,8 +711,7 @@
     loads[2].wait()
     loads[3].wait()
     shared_chunk(z, True)
-    got(halved(XB, z, 0), xy_r.at[0, z])
-    got(halved(YB, z, 1), xy_r.at[1, z])
+    side_arrival(z, 0)
     remote(halved(XB, z, 0), halved(DB, z, 0), dr_s.at[0], dr_r.at[0], yn)
     remote(halved(YB, z, 1), halved(DB, z, 1), dr_s.at[1], dr_r.at[1], xn)
     at_middle(lambda: [z_arrival(0, nears[j], 1) for j in (0, 1)])
@@ -677,10 +732,7 @@
     at_middle(lambda: to_xy(nears[2]))
     attend_first(0)
     attend_first(1)
-    got(halved(XB, z, 1), xy_r.at[0, chips])
-    got(halved(YB, z, 0), xy_r.at[1, chips])
-    to_pair(piece(XB, z, c), XB, z)
-    to_pair(piece(YB, z, c), YB, z)
+    side_arrival(z, 1)
     at_edge(lambda: arrivals(0, 1))
     at_edge(lambda: to_xy(nears[1]))
     got(halved(DB, z, 0), dr_r.at[0])
@@ -708,74 +760,79 @@
     finish_head(0)
     finish_head(1)
     mine = ho.at[:, cols(c, vwide)]
-    remote(mine, mine, h_s.at[5], h_r.at[5], pt)
+    remote(mine, mine, h_s.at[6], h_r.at[6], pt)
     at_middle(lambda: [z_arrival(1, nears[j], 1) for j in (0, 1)])
     expert_chunk(DB, z, True)
     expert_chunk(OWN, nears[2], False)
-    activate(OWN, acc.at[pl.ds(OWN * rows, rows), :], hidden, hid.at[OWN], OWN)
+    expert_activate(0, rows, 0)
     shared_chunk(nears[2], False)
-    activate(OWN, sacc, shared, shid, 4)
+    activate(0, rows, sacc, shared, shid, 0, 5)
     at_edge(lambda: arrivals(1, 0))
-    side_arrival(nears[0])
+    side_arrival(nears[0], 0)
+    side_arrival(nears[0], 1)
     for p in range(chips):
         loads[5 + p].wait()
         got(ow.at[cols(1 - c, vwide), pl.ds(p * part, part)], w_r.at[0, p])
-    got(ho.at[:, cols(1 - c, vwide)], h_r.at[5])
+    got(ho.at[:, cols(1 - c, vwide)], h_r.at[6])
     for j in range(chips):
         span = cols(fars[j], part)
         macc[:, span] = mm(ho[...], ow[:, span])
 
-    def z_send(kind, j, p, value_of):
+    def z_send(kind, j, p, h, value_of):
         upstream = ((p > z) & has_l) | ((p < z) & has_r)
-        slot = zout.at[kind, j]
+        at = pl.ds(h * half, half)
+        slot = zout.at[kind, j, at]
 
         @pl.when(upstream)
         def _():
-            got(zin.at[kind, p], z_r.at[kind, p])
-            zout[kind, j] = low(value_of() + f32(zin[kind, p]))
+            got(zin.at[kind, p, at], z_r.at[kind, p, h])
+            zout[kind, j, at] = low(value_of(at) + f32(zin[kind, p, at]))
 
         @pl.when(jnp.logical_not(upstream))
         def _():
-            zout[kind, j] = low(value_of())
+            zout[kind, j, at] = low(value_of(at))
 
         @pl.when(p > z)
         def _():
-            remote(slot, zin.at[kind, p], z_s.at[kind, j], z_r.at[kind, p], zr)
+            remote(slot, zin.at[kind, p, at], z_s.at[kind, j, h], z_r.at[kind, p, h], zr)
 
         @pl.when((p < z) & (p != z - 1))
         def _():
-            remote(slot, zin.at[kind, p], z_s.at[kind, j], z_r.at[kind, p], zl)
+            remote(slot, zin.at[kind, p, at], z_s.at[kind, j, h], z_r.at[kind, p, h], zl)
 
         @pl.when((p < z) & (p == z - 1))
         def _():
-            remote(slot, zin.at[kind, chips], z_s.at[kind, j], z_r.at[kind, chips], zl)
-
-    def z_finish(kind, value):
+            remote(slot, zin.at[kind, chips, at], z_s.at[kind, j, h], z_r.at[kind, chips, h], zl)
+
+    def z_finish(kind, value_of):
         target = (mix_ref, out_ref)[kind]
-
-        @pl.when(has_l)
-        def _():
-            got(zin.at[kind, z], z_r.at[kind, z])
-
-        @pl.when(has_r)
-        def _():
-            got(zin.at[kind, chips], z_r.at[kind, chips])
-
-        @pl.when(has_l & has_r)
-        def _():
-            target[...] = low(value + f32(zin[kind, z]) + f32(zin[kind, chips]))
-
-        @pl.when(jnp.logical_not(has_l))
-        def _():
-            target[...] = low(value + f32(zin[kind, chips]))
-
-        @pl.when(jnp.logical_not(has_r))
-        def _():
-            target[...] = low(value + f32(zin[kind, z]))
+        for h in range(2):
+            at = pl.ds(h * half, half)
+
+            @pl.when(has_l)
+            def _():
+                got(zin.at[kind, z, at], z_r.at[kind, z, h])
+
+            @pl.when(has_r)
+            def _():
+                got(zin.at[kind, chips, at], z_r.at[kind, chips, h])
+
+            @pl.when(has_l & has_r)
+            def _():
+                target[at] = low(value_of(at) + f32(zin[kind, z, at]) + f32(zin[kind, chips, at]))
+
+            @pl.when(jnp.logical_not(has_l))
+            def _():
+                target[at] = low(value_of(at) + f32(zin[kind, chips, at]))
+
+            @pl.when(jnp.logical_not(has_r))
+            def _():
+                target[at] = low(value_of(at) + f32(zin[kind, z, at]))
 
     def mixer_send(j):
         p = fars[j]
-        z_send(0, j, p, lambda: macc[:, cols(p, part)])
+        for h in range(2):
+            z_send(0, j, p, h, lambda at: macc[at, cols(p, part)])
 
     at_edge(lambda: [mixer_send(j) for j in range(chips - 1)])
     at_middle(lambda: z_arrival(1, nears[2], 0))
@@ -784,100 +841,143 @@
         loads[5 + 2 * chips + p].wait()
         got(sd.at[cols(1 - c, shared), pl.ds(p * part, part)], w_r.at[1, p])
         got(dw.at[cols(1 - c, hidden), pl.ds(p * part, part)], w_r.at[2, p])
-    got(hid.at[OWN, :, cols(1 - c, hidden)], h_r.at[OWN])
-    got(shid.at[:, cols(1 - c, shared)], h_r.at[4])
     got(shtab.at[DB], sh_r.at[2])
     for block in range(4):
         line = jnp.sum(jnp.where(expert_id == e, shtab[block], 0.0), axis=0, keepdims=True)
-        shcol[block] = jnp.broadcast_to(line, (128, rows)).T
+        column = jnp.broadcast_to(line, (128, rows)).T
+        for h in range(2):
+            shcol[pl.ds(base(block, h), half), :] = column[h * half : (h + 1) * half]
+    expert_chunk(XB, nears[0], False, 3)
+    at_middle(lambda: z_arrival(1, nears[2], 1))
+    at_edge(lambda: arrivals(1, 1))
+    side_arrival(nears[1], 0)
+    side_arrival(nears[1], 1)
+    EARLY, X_LATE, Y_LATE, FAR = rows + half, rows, 2 * rows + half, 3 * rows
+    expert_rows(XB * rows, 3 * rows, 2 * nears[1] + c, part)
+    paired(DB, nears[1])
+    for i in range(2):
+        for order in range(2):
+            paired_half(i, order, nears[1])
+    expert_rows(XB * rows, 3 * rows, 2 * nears[1] + 1 - c, part)
+    side_arrival(nears[2], 0)
+    expert_rows(EARLY, rows, 2 * nears[2] + c, part)
+    paired_half(0, 0, nears[2])
+    paired_half(1, 0, nears[2])
+    expert_rows(EARLY, rows, 2 * nears[2] + 1 - c, part)
+    expert_activate(EARLY, rows, 1)
+    at_edge(lambda: arrivals(1, 2))
+    side_arrival(nears[2], 1)
+
+    def down(start, count, p):
+        span = pl.ds(start, count)
+        return mm(hid[span, :], dw[:, cols(p, part)]) * shcol[span, 0:1]
 
     def own_down(p, carry):
         span = cols(p, part)
-        oacc[:, span] = mm(hid[OWN], dw[:, span]) * shcol[OWN, :, 0:1] + mm(shid[...], sd[:, span])
+        oacc[:, span] = down(0, rows, p) + mm(shid[...], sd[:, span])
         return carry
 
-    lax.fori_loop(0, chips, own_down, 0)
-    at_middle(lambda: z_arrival(1, nears[2], 1))
-    at_edge(lambda: arrivals(1, 1))
-    side_arrival(nears[1])
-    expert_chunk(XB, nears[0], False, 3)
-    expert_chunk(XB, nears[1], False, 3)
-    at_edge(lambda: arrivals(1, 2))
-    side_arrival(nears[2])
-    expert_half(DB, nears[2], c)
-    expert_half(XB, nears[2], c, 2)
-    expert_half(DB, nears[2], 1 - c)
-    activate(DB, acc.at[pl.ds(DB * rows, rows), :], hidden, hid.at[DB], DB)
-    expert_half(XB, nears[2], 1 - c, 2)
-
-    def down(block, p):
-        return mm(hid[block], dw[:, cols(p, part)]) * shcol[block, :, 0:1]
-
     top, rest = pl.ds(0, half), pl.ds(half, half)
-    sides = ((0, XB, 0, 1, xn), (1, YB, 1, 0, yn))
+    sides = ((0, X_LATE, 0, 1, xn), (1, Y_LATE, 1, 0, yn))
 
     def far_share(j):
         span = cols(fars[j], part)
-        dsend[:, span] = low(down(DB, fars[j]))
+        dsend[:, span] = low(down(FAR, rows, fars[j]))
         remote(dsend.at[top, span], din.at[0, :, span], d_s.at[0, j], d_r.at[0, j], xn)
         remote(dsend.at[rest, span], din.at[1, :, span], d_s.at[1, j], d_r.at[1, j], yn)
 
     def early_share(j):
         span = cols(fars[j], part)
-        for i, block, now, later, dev in sides:
-            value = down(block, fars[j])
-            esend[i, :, span] = low(value[now * half : (now + 1) * half])
-            late[i, :, span] = value[later * half : (later + 1) * half]
+        value = low(down(EARLY, rows, fars[j]))
+        for i, start, now, later, dev in sides:
+            esend[i, :, span] = value[i * half : (i + 1) * half]
             target = xyin.at[i, pl.ds(now * half, half), span]
             remote(esend.at[i, :, span], target, e_s.at[i, 0, j], e_r.at[i, 0, j], dev)
 
     def late_share(j):
         span = cols(fars[j], part)
-        for i, block, now, later, dev in sides:
+        for i, start, now, later, dev in sides:
+            late[i] = down(start, half, fars[j])
+        for i, start, now, later, dev in sides:
             got(din.at[1 - i, :, span], d_r.at[1 - i, j])
-            lsend[i, :, span] = low(late[i, :, span] + f32(din[1 - i, :, span]))
+            lsend[i, :, span] = low(late[i] + f32(din[1 - i, :, span]))
             target = xyin.at[i, pl.ds(later * half, half), span]
             remote(lsend.at[i, :, span], target, e_s.at[i, 1, j], e_r.at[i, 1, j], dev)
 
-    def total_share(j):
+    def total(j):
         span = cols(fars[j], part)
-        for i, block, now, later, dev in sides:
+        return lambda at: oacc[at, span] + f32(xyin[0, at, span]) + f32(xyin[1, at, span])
+
+    def total_ready(j):
+        span = cols(fars[j], part)
+        for i, start, now, later, dev in sides:
             got(xyin.at[i, pl.ds(now * half, half), span], e_r.at[i, 0, j])
             got(xyin.at[i, pl.ds(later * half, half), span], e_r.at[i, 1, j])
 
-        def total():
-            return oacc[:, span] + f32(xyin[0, :, span]) + f32(xyin[1, :, span])
-
-        if j < chips - 1:
-            z_send(1, j, fars[j], total)
-        else:
-            z_finish(1, total())
-
-    got(hid.at[DB, :, cols(1 - c, hidden)], h_r.at[DB])
+    def total_half(j, h):
+        z_send(1, j, fars[j], h, total(j))
+
+    def total_share(j):
+        total_ready(j)
+        total_half(j, 0)
+        total_half(j, 1)
+
+    expert_rows(Y_LATE, half + rows, 2 * nears[2] + c, part)
+    expert_hidden(EARLY, rows, 1)
+    early_share(0)
+    early_share(1)
+    paired(DB, nears[2])
+    paired_half(1, 1, nears[2])
+    expert_rows(Y_LATE, half + rows, 2 * nears[2] + 1 - c, part)
+    expert_activate(FAR, rows, 2)
+    expert_activate(Y_LATE, half, 4)
+    expert_rows(X_LATE, half, 2 * nears[2] + c, part)
+    paired_half(0, 1, nears[2])
+    expert_rows(X_LATE, half, 2 * nears[2] + 1 - c, part)
+    expert_activate(X_LATE, half, 3)
+    expert_hidden(FAR, rows, 2)
     far_share(0)
-    activate(XB, acc.at[pl.ds(XB * rows, rows), :], hidden, hid.at[XB], XB)
-    activate(YB, acc.at[pl.ds(YB * rows, rows), :], hidden, hid.at[YB], YB)
-    got(hid.at[XB, :, cols(1 - c, hidden)], h_r.at[XB])
-    got(hid.at[YB, :, cols(1 - c, hidden)], h_r.at[YB])
-    early_share(0)
     far_share(1)
     at_middle(lambda: mixer_send(0))
+    expert_hidden(0, rows, 0)
+    got(shid.at[:, cols(1 - c, shared)], h_r.at[5])
+    lax.fori_loop(0, chips, own_down, 0)
+    expert_hidden(X_LATE, half, 3)
+    expert_hidden(Y_LATE, half, 4)
     late_share(0)
-    early_share(1)
+    at_middle(lambda: mixer_send(1))
     far_share(2)
-    at_middle(lambda: mixer_send(1))
     late_share(1)
     early_share(2)
+    at_middle(lambda: mixer_send(2))
+    at_edge(lambda: total_share(0))
+    late_share(2)
     far_share(3)
-    at_middle(lambda: mixer_send(2))
-    total_share(0)
-    late_share(2)
+    at_middle(lambda: total_share(0))
+    at_edge(lambda: total_share(1))
     early_share(3)
-    total_share(1)
+    at_edge(lambda: total_share(2))
+
+    def middle_first():
+        total_ready(1)
+        total_half(1, 0)
+        total_ready(2)
+        total_half(2, 0)
+
+    def middle_second():
+        total_half(1, 1)
+        total_half(2, 1)
+
+    at_middle(middle_first)
     late_share(3)
-    z_finish(0, macc[:, cols(z, part)])
-    total_share(2)
-    total_share(3)
+    at_middle(middle_second)
+    z_finish(0, lambda at: macc[at, cols(z, part)])
+    mix_out = pltpu.make_async_copy(mix_ref, mix_hbm, in_l.at[7])
+    mix_out.start()
+    total_ready(3)
+    z_finish(1, total(3))
+    routed_out = pltpu.make_async_copy(out_ref, out_hbm, in_l.at[8])
+    routed_out.start()
 
     for kind, block in ((0, OWN), (1, DB)):
         for s in range(chips):
@@ -892,14 +992,13 @@
                 for h in range(2):
                     sent(halved(block, s, h), ag_s.at[kind, 1, s, h])
 
-    for i in range(2):
-        sent(halved(OWN, z, 0), xy_s.at[i, z])
-        sent(halved(OWN, z, 0), xy_s.at[i, chips])
-        for j in range(chips - 1):
-            sent(piece(OWN, nears[j], c), xy_s.at[i, nears[j]])
     for s in range(chips):
-        for block in range(4):
-            sent(piece(block, s, c), pt_s.at[block, s])
+        for i in range(2):
+            for order in range(2):
+                sent(halved(OWN, s, 0), xy_s.at[i, s, order])
+                sent(halved(OWN, s, 0), pt_s.at[(XB, YB)[i], s, order])
+        for block in (OWN, DB):
+            sent(piece(block, s, c), pt_s.at[block, s, 0])
     for i in range(2):
         sent(halved(DB, z, i), dr_s.at[i])
         sent(kv_rows(OWN, 0, rows), kv_s.at[i])
@@ -909,26 +1008,33 @@
         for p in range(chips):
             src, dst, depth = downs[i]
             sent(dst.at[cols(c, depth), pl.ds(p * part, part)], w_s.at[i, p])
-    for block in range(4):
-        sent(hid.at[block, :, cols(c, hidden)], h_s.at[block])
-    sent(shid.at[:, cols(c, shared)], h_s.at[4])
-    sent(ho.at[:, cols(c, vwide)], h_s.at[5])
+    for count, index in ((rows, 0), (rows, 1), (rows, 2), (half, 3), (half, 4)):
+        sent(hid.at[pl.ds(0, count), cols(c, hidden)], h_s.at[index])
+    sent(shid.at[:, cols(c, shared)], h_s.at[5])
+    sent(ho.at[:, cols(c, vwide)], h_s.at[6])
     for i in range(2):
         for j in range(chips):
             sent(dsend.at[top, pl.ds(j * part, part)], d_s.at[i, j])
             sent(esend.at[i, :, pl.ds(j * part, part)], e_s.at[i, 0, j])
             sent(lsend.at[i, :, pl.ds(j * part, part)], e_s.at[i, 1, j])
         for j in range(chips - 1):
-            sent(zout.at[i, j], z_s.at[i, j])
-
-
-def emit_kernel(mixed_ref, routed_ref, mix_hbm, out_hbm, sems):
-    first = pltpu.make_async_copy(mixed_ref, mix_hbm, sems.at[0])
-    second = pltpu.make_async_copy(routed_ref, out_hbm, sems.at[1])
-    first.start()
-    second.start()
-    first.wait()
-    second.wait()
+            for h in range(2):
+                sent(zout.at[i, j, pl.ds(0, half)], z_s.at[i, j, h])
+    mix_out.wait()
+    routed_out.wait()
+
+
+def emit_kernel(mixed_hbm, routed_hbm, mix_hbm, out_hbm, mixed, routed, sems):
+    pairs = ((mixed_hbm, mixed, mix_hbm), (routed_hbm, routed, out_hbm))
+    loads = [pltpu.make_async_copy(src, held, sems.at[i]) for i, (src, held, _) in enumerate(pairs)]
+    stores = [pltpu.make_async_copy(held, dst, sems.at[2 + i]) for i, (_, held, dst) in enumerate(pairs)]
+    for load in loads:
+        load.start()
+    for load, store in zip(loads, stores):
+        load.wait()
+        store.start()
+    for store in stores:
+        store.wait()
 
 
 def rotation_table(positions, key_width):
@@ -970,7 +1076,6 @@
     local_heads = diff_lambda.shape[0]
     half, mine = rows // 2, width // 2
     table = jnp.asarray(rotation_table(groups * rows, kwide // (2 * local_heads)))
-    vmem = pl.BlockSpec(memory_space=pltpu.VMEM)
     smem = pl.BlockSpec(memory_space=pltpu.SMEM)
     hbm = pl.BlockSpec(memory_space=pl.ANY)
     dma = pltpu.SemaphoreType.DMA
@@ -978,9 +1083,11 @@
     mixed, routed = pl.pallas_call(
         functools.partial(layer_kernel, chips),
         out_shape=(out, out),
-        in_specs=[vmem, vmem, vmem, smem, vmem, vmem, vmem, vmem] + [hbm] * 8,
-        out_specs=(vmem, vmem),
+        in_specs=[smem] + [hbm] * 15,
+        out_specs=(hbm, hbm),
         scratch_shapes=[
+            pltpu.VMEM((rows, part), BF16),
+            pltpu.VMEM((rows, part), BF16),
             pltpu.VMEM((groups * rows, width), BF16),
             pltpu.VMEM((width, 2 * hidden), BF16),
             pltpu.VMEM((2 * hidden, mine), BF16),
@@ -988,16 +1095,21 @@
             pltpu.VMEM((2 * shared, mine), BF16),
             pltpu.VMEM((2 * vwide, mine), BF16),
             pltpu.VMEM((rows, 256), F32),
+            pltpu.VMEM(query_heads.shape, BF16),
+            pltpu.VMEM(key_heads.shape, BF16),
+            pltpu.VMEM((1, sub_gain.shape[0]), F32),
+            pltpu.VMEM(routes.shape[::-1], routes.dtype),
+            pltpu.VMEM(routes.shape[::-1], F32),
             pltpu.VMEM((groups * rows, 2 * hidden), F32),
             pltpu.VMEM((rows, 2 * shared), F32),
             pltpu.VMEM((groups * rows, 128), F32),
-            pltpu.VMEM((groups, rows, 2 * hidden), BF16),
+            pltpu.VMEM((groups * rows, 2 * hidden), BF16),
             pltpu.VMEM((rows, 2 * shared), BF16),
             pltpu.VMEM((rows, mine), F32),
             pltpu.VMEM((rows, mine), BF16),
             pltpu.VMEM((2, half, mine), BF16),
             pltpu.VMEM((2, half, mine), BF16),
-            pltpu.VMEM((2, half, mine), F32),
+            pltpu.VMEM((2, half, part), F32),
             pltpu.VMEM((2, half, mine), BF16),
             pltpu.VMEM((2, rows, mine), BF16),
             pltpu.VMEM((2, chips + 1, rows, part), BF16),
@@ -1013,40 +1125,41 @@
             pltpu.VMEM((rows, 128), F32),
             pltpu.VMEM((rows, 2 * vwide), BF16),
             pltpu.VMEM((groups, 8, rows), F32),
-            pltpu.VMEM((groups, rows, 128), F32),
+            pltpu.VMEM((groups * rows, 128), F32),
             dma((5 + 3 * chips,)),
             dma((3, chips)),
             dma((3, chips)),
             dma((2, 2, chips, 2)),
             dma((2, chips, 2)),
-            dma((2, chips + 1)),
-            dma((2, chips + 1)),
+            dma((2, chips, 2)),
+            dma((2, chips, 2)),
             dma((2,)),
             dma((2,)),
-            dma((4, chips)),
-            dma((4, chips)),
+            dma((4, chips, 2)),
+            dma((4, chips, 2)),
             dma((4,)),
             dma((4,)),
             dma((3,)),
             dma((3,)),
-            dma((6,)),
-            dma((6,)),
+            dma((7,)),
+            dma((7,)),
             dma((2, chips)),
             dma((2, chips)),
             dma((2, 2, chips)),
             dma((2, 2, chips)),
-            dma((2, chips - 1)),
-            dma((2, chips + 1)),
+            dma((2, chips - 1, 2)),
+            dma((2, chips + 1, 2)),
+            dma((9,)),
         ],
         compiler_params=pltpu.CompilerParams(
             collective_id=0, has_side_effects=True, vmem_limit_bytes=67043328
         ),
         name="layer",
     )(
+        diff_lambda,
         query_heads,
         key_heads,
         value_heads,
-        diff_lambda,
         sub_gain[None, :],
         routed_input,
         routes.T,
@@ -1063,9 +1176,9 @@
     return pl.pallas_call(
         emit_kernel,
         out_shape=(out, out),
-        in_specs=[vmem, vmem],
+        in_specs=[hbm, hbm],
         out_specs=(hbm, hbm),
-        scratch_shapes=[dma((2,))],
+        scratch_shapes=[pltpu.VMEM((rows, part), BF16), pltpu.VMEM((rows, part), BF16), dma((4,))],
         name="emit",
     )(mixed, routed)
 

time: 88.4 us -> 84.9 us (0.960)
  Pallas kernels: 86.6 us -> 84 us
    pallas_call x1, Pallas kernels: 84.8 us -> 82.2 us  [kernel_body(): pl.pallas_call(functools.partial(layer_kernel, chips), out_shape=(out, ou...]
where the time goes in v3:
time: 84.9 us; the launch traced here: 84.8 us
  Pallas kernels  84 us (99%)
    pallas_call x1, Pallas kernels, kernel_body(): pl.pallas_call(functools.partial(layer_kernel, chips), out_shape=(out, ou...  82.2 us
    pallas_call x1, Pallas kernels, kernel_body(): pl.pallas_call(emit_kernel, out_shape=(out, out), in_specs=[hbm, hbm], ou...  1.77 us

profile of v3, /device:TPU:0, one launch (start us, length us, event | category | flops | bytes accessed | tf_op | source)
XLA Modules:
  0.0 84.8 jit_solution(11818827488254396647)
XLA Ops:
  0.6 82.2 %layer.1 = (bf16[256,512]{1,0:T(8,128)(2,1)}, bf16[256,512]{1,0:T(8,128)(2,1)}) custom-call(f32[2]{0:T(128)} %lam_ref.1, bf16[256,256]{1,0:T(8,128)(2,1)} %q_hbm.1, bf16[256,256]{1,0:T(8,128)(2,1)} %k_hbm.1, bf16[256,256]{1,0:T(8,128)(2,1)} %v_hbm.1, f32[1,128]{1,0:T(1,128)} %bitcast.11, bf16[256,512]{1,0:T(8,128)(2,1)} %x_hbm.1, s32[2,256]{1,0:T(2,128)} %bitcast.9, ...), custom_call_target="tpu_custom_call" | custom-call | tf_op jit(solution)/shard_map/layer/pallas_call | solution.py:1083
  82.8 1.8 %emit.1 = (bf16[256,512]{1,0:T(8,128)(2,1)}, bf16[256,512]{1,0:T(8,128)(2,1)}) custom-call(bf16[256,512]{1,0:T(8,128)(2,1)} %get-tuple-element.4.mixed_hbm, bf16[256,512]{1,0:T(8,128)(2,1)} %get-tuple-element.5.routed_hbm), custom_call_target="tpu_custom_call" | custom-call | tf_op jit(solution)/shard_map/emit/pallas_call | solution.py:1176

commit v4 on v3

--- a/solution.py
+++ b/solution.py
@@ -427,7 +427,7 @@
                 pltpu.make_async_copy(
                     src.at[:, cols(2 * p + c, part)],
                     dst.at[cols(c, depth), pl.ds(p * part, part)],
-                    w_l.at[5 + i * chips + p],
+                    w_l.at[5 + i],
                 )
             )
     own_rows = pl.ds(0, rows)
@@ -452,22 +452,25 @@
         return xall.at[pl.ds(block * rows, rows), cols(2 * s + core, part)]
 
     def base(block, h):
-        return block * rows + (h if block in (OWN, DB) else 1 - h) * half
+        if block in (OWN, DB):
+            return block * rows + h * half
+        early = h == (0 if block == XB else 1)
+        return (rows if early else 2 * rows) + (0 if block == XB else half)
 
     def halved(block, s, h, core=None):
         return xall.at[pl.ds(base(block, h), half), cols(2 * s + (c if core is None else core), part)]
 
-    def z_forward(src, kind, block, s, h, right, left):
+    def z_forward(src, kind, block, s, h, right, left, slot=None):
         @pl.when(right)
         def _():
-            remote(src, halved(block, s, h), ag_s.at[kind, 0, s, h], ag_r.at[kind, s, h], zr)
+            remote(src, halved(block, s, h), ag_s.at[kind, s, h], ag_r.at[kind, s, h], zr)
 
         @pl.when(left)
         def _():
-            remote(src, halved(block, s, h), ag_s.at[kind, 1, s, h], ag_r.at[kind, s, h], zl)
+            remote(src, halved(block, s, h), ag_s.at[kind, s if slot is None else slot, h], ag_r.at[kind, s, h], zl)
 
     def to_pair(src, block, s):
-        remote(src, piece(block, s, c), pt_s.at[block, s, 0], pt_r.at[block, s, 0], pt)
+        remote(src, piece(block, s, c), pt_s.at[0], pt_r.at[block, s], pt)
 
     def half_of(i, order):
         return order if i == 0 else 1 - order
@@ -475,30 +478,28 @@
     def to_side(i, order, s, src):
         block, dev = ((XB, xn), (YB, yn))[i]
         target = halved(block, s, half_of(i, order))
-        remote(src, target, xy_s.at[i, s, order], xy_r.at[i, s, order], dev)
+        remote(src, target, xy_s.at[i], xy_r.at[order, s], dev)
 
     def own_half(i, order):
         to_side(i, order, z, halved(OWN, z, half_of(i, order)))
 
-    def to_xy(s):
-        for order in range(2):
-            for i in range(2):
-                to_side(i, order, s, halved(OWN, s, half_of(i, order)))
-
-    def side_half(i, order, s, core=None):
-        return halved((XB, YB)[i], s, half_of(i, order), core)
+    def to_xy(s, order):
+        for i in range(2):
+            to_side(i, order, s, halved(OWN, s, half_of(i, order)))
+
+    def side_rows(order, s, core):
+        return xall.at[pl.ds((1 + order) * rows, rows), cols(2 * s + core, part)]
 
     def side_arrival(s, order):
-        for i, block in ((0, XB), (1, YB)):
-            mine = side_half(i, order, s)
-            got(mine, xy_r.at[i, s, order])
-            remote(mine, mine, pt_s.at[block, s, order], pt_r.at[block, s, order], pt)
+        mine = side_rows(order, s, c)
+        got(mine, xy_r.at[order, s])
+        remote(mine, mine, pt_s.at[0], pt_r.at[1 + order, s], pt)
 
     def paired(block, s):
-        got(piece(block, s, 1 - c), pt_r.at[block, s, 0])
-
-    def paired_half(i, order, s):
-        got(side_half(i, order, s, 1 - c), pt_r.at[(XB, YB)[i], s, order])
+        got(piece(block, s, 1 - c), pt_r.at[block, s])
+
+    def paired_sides(order, s):
+        got(side_rows(order, s, 1 - c), pt_r.at[1 + order, s])
 
     inputs[0].wait()
     loads[0].start()
@@ -506,7 +507,7 @@
     pl.semaphore_wait(barrier, 3 + has_r.astype(jnp.int32) + has_l.astype(jnp.int32))
 
     for h in range(2):
-        z_forward(halved(OWN, z, h), 0, OWN, z, h, has_r, has_l)
+        z_forward(halved(OWN, z, h), 0, OWN, z, h, has_r, has_l, chips)
     own_half(0, 0)
     own_half(1, 0)
     to_pair(piece(OWN, z, c), OWN, z)
@@ -521,7 +522,7 @@
         table = table + jnp.where(routes[k : k + 1, :] == expert_id, weights[k : k + 1, :], 0.0)
     shtab[OWN] = table
     remote(shtab.at[OWN], shtab.at[XB], sh_s.at[0], sh_r.at[0], xn)
-    remote(shtab.at[OWN], shtab.at[YB], sh_s.at[1], sh_r.at[1], yn)
+    remote(shtab.at[OWN], shtab.at[YB], sh_s.at[0], sh_r.at[0], yn)
 
     for copy in inputs[1:4]:
         copy.wait()
@@ -548,7 +549,7 @@
         return kv.at[pl.ds(block * rows + start, count), :]
 
     remote(kv_rows(OWN, 0, rows), kv_rows(XB, 0, rows), kv_s.at[0], kv_r.at[0], xn)
-    remote(kv_rows(OWN, 0, rows), kv_rows(YB, 0, rows), kv_s.at[1], kv_r.at[1], yn)
+    remote(kv_rows(OWN, 0, rows), kv_rows(YB, 0, rows), kv_s.at[0], kv_r.at[0], yn)
 
     own_half(0, 1)
     own_half(1, 1)
@@ -561,10 +562,16 @@
             remote(
                 src.at[:, cols(2 * p + 1 - c, part)],
                 dst.at[cols(c, depth), pl.ds(p * part, part)],
-                w_s.at[i, p],
-                w_r.at[i, p],
+                w_s.at[i],
+                w_r.at[i],
                 pt,
             )
+
+    def down_ready(i):
+        src, dst, depth = downs[i]
+        mine = dst.at[cols(c, depth), :]
+        pltpu.make_async_copy(mine, mine, w_l.at[5 + i]).wait()
+        got(dst.at[cols(1 - c, depth), :], w_r.at[i])
 
     def chunk(start, count, at, depth, first, weight, target, width):
         tiles = target.shape[-1] // width
@@ -597,8 +604,7 @@
             if b in (OWN, DB):
                 paired(b, s)
             else:
-                for order in range(2):
-                    paired_half(b - XB, order, s)
+                paired_sides(b - XB, s)
         expert_rows(block * rows, count * rows, s, wide, first)
 
     def shared_chunk(s, first):
@@ -612,7 +618,7 @@
         up = source[span, width:] * factor
         target[span, cols(c, width)] = low(gate / (1.0 + jnp.exp(-gate)) * up)
         mine = target.at[span, cols(c, width)]
-        remote(mine, mine, h_s.at[index], h_r.at[index], pt)
+        remote(mine, mine, h_s.at[0 if index < 4 else 1], h_r.at[index], pt)
 
     def expert_activate(start, count, index):
         activate(start, count, acc, hidden, hid, start, index)
@@ -713,32 +719,29 @@
     shared_chunk(z, True)
     side_arrival(z, 0)
     remote(halved(XB, z, 0), halved(DB, z, 0), dr_s.at[0], dr_r.at[0], yn)
-    remote(halved(YB, z, 1), halved(DB, z, 1), dr_s.at[1], dr_r.at[1], xn)
+    remote(halved(YB, z, 1), halved(DB, z, 1), dr_s.at[0], dr_r.at[0], xn)
     at_middle(lambda: [z_arrival(0, nears[j], 1) for j in (0, 1)])
     at_edge(lambda: arrivals(0, 0))
     at_middle(lambda: z_arrival(0, nears[2], 0))
     expert_chunk(OWN, nears[0], False)
     shared_chunk(nears[0], False)
-    got(kv_rows(XB, 0, rows), kv_r.at[0])
-    got(kv_rows(YB, 0, rows), kv_r.at[1])
-    remote(kv_rows(XB, 0, half), kv_rows(DB, 0, half), kv_s.at[2], kv_r.at[2], yn)
-    remote(kv_rows(YB, half, half), kv_rows(DB, half, half), kv_s.at[3], kv_r.at[3], xn)
-    got(shtab.at[XB], sh_r.at[0])
-    got(shtab.at[YB], sh_r.at[1])
-    remote(shtab.at[XB], shtab.at[DB], sh_s.at[2], sh_r.at[2], yn)
-    to_xy(nears[0])
-    at_middle(lambda: to_xy(nears[1]))
+    got(kv_rows(XB, 0, 2 * rows), kv_r.at[0])
+    remote(kv_rows(XB, 0, half), kv_rows(DB, 0, half), kv_s.at[0], kv_r.at[1], yn)
+    remote(kv_rows(YB, half, half), kv_rows(DB, half, half), kv_s.at[0], kv_r.at[1], xn)
+    got(shtab.at[pl.ds(XB, 2)], sh_r.at[0])
+    remote(shtab.at[XB], shtab.at[DB], sh_s.at[0], sh_r.at[1], yn)
+    to_xy(nears[0], 0)
+    at_middle(lambda: to_xy(nears[1], 0))
     at_middle(lambda: z_arrival(0, nears[2], 1))
-    at_middle(lambda: to_xy(nears[2]))
+    at_middle(lambda: to_xy(nears[2], 0))
     attend_first(0)
     attend_first(1)
     side_arrival(z, 1)
     at_edge(lambda: arrivals(0, 1))
-    at_edge(lambda: to_xy(nears[1]))
-    got(halved(DB, z, 0), dr_r.at[0])
-    got(halved(DB, z, 1), dr_r.at[1])
+    at_edge(lambda: to_xy(nears[1], 0))
+    got(piece(DB, z, c), dr_r.at[0])
     for h in range(2):
-        z_forward(halved(DB, z, h), 1, DB, z, h, has_r, has_l)
+        z_forward(halved(DB, z, h), 1, DB, z, h, has_r, has_l, chips)
     to_pair(piece(DB, z, c), DB, z)
     give_down(0)
     attend_first(2)
@@ -748,32 +751,31 @@
 
     def last_own():
         arrivals(0, 2)
-        to_xy(nears[2])
+        to_xy(nears[2], 0)
 
     at_edge(last_own)
+    for j in range(chips - 1):
+        to_xy(nears[j], 1)
     give_down(1)
     give_down(2)
     expert_chunk(XB, z, True, 2)
     at_middle(lambda: [z_arrival(1, nears[j], 0) for j in (0, 1)])
-    got(kv_rows(DB, 0, half), kv_r.at[2])
-    got(kv_rows(DB, half, half), kv_r.at[3])
+    got(kv_rows(DB, 0, rows), kv_r.at[1])
     finish_head(0)
     finish_head(1)
     mine = ho.at[:, cols(c, vwide)]
-    remote(mine, mine, h_s.at[6], h_r.at[6], pt)
+    remote(mine, mine, h_s.at[2], h_r.at[5], pt)
     at_middle(lambda: [z_arrival(1, nears[j], 1) for j in (0, 1)])
+    side_arrival(nears[0], 0)
     expert_chunk(DB, z, True)
     expert_chunk(OWN, nears[2], False)
     expert_activate(0, rows, 0)
     shared_chunk(nears[2], False)
-    activate(0, rows, sacc, shared, shid, 0, 5)
+    activate(0, rows, sacc, shared, shid, 0, 4)
     at_edge(lambda: arrivals(1, 0))
-    side_arrival(nears[0], 0)
-    side_arrival(nears[0], 1)
-    for p in range(chips):
-        loads[5 + p].wait()
-        got(ow.at[cols(1 - c, vwide), pl.ds(p * part, part)], w_r.at[0, p])
-    got(ho.at[:, cols(1 - c, vwide)], h_r.at[6])
+    side_arrival(nears[1], 0)
+    down_ready(0)
+    got(ho.at[:, cols(1 - c, vwide)], h_r.at[5])
     for j in range(chips):
         span = cols(fars[j], part)
         macc[:, span] = mm(ho[...], ow[:, span])
@@ -794,15 +796,15 @@
 
         @pl.when(p > z)
         def _():
-            remote(slot, zin.at[kind, p, at], z_s.at[kind, j, h], z_r.at[kind, p, h], zr)
+            remote(slot, zin.at[kind, p, at], z_s.at[kind], z_r.at[kind, p, h], zr)
 
         @pl.when((p < z) & (p != z - 1))
         def _():
-            remote(slot, zin.at[kind, p, at], z_s.at[kind, j, h], z_r.at[kind, p, h], zl)
+            remote(slot, zin.at[kind, p, at], z_s.at[kind], z_r.at[kind, p, h], zl)
 
         @pl.when((p < z) & (p == z - 1))
         def _():
-            remote(slot, zin.at[kind, chips, at], z_s.at[kind, j, h], z_r.at[kind, chips, h], zl)
+            remote(slot, zin.at[kind, chips, at], z_s.at[kind], z_r.at[kind, chips, h], zl)
 
     def z_finish(kind, value_of):
         target = (mix_ref, out_ref)[kind]
@@ -836,37 +838,30 @@
 
     at_edge(lambda: [mixer_send(j) for j in range(chips - 1)])
     at_middle(lambda: z_arrival(1, nears[2], 0))
-    for p in range(chips):
-        loads[5 + chips + p].wait()
-        loads[5 + 2 * chips + p].wait()
-        got(sd.at[cols(1 - c, shared), pl.ds(p * part, part)], w_r.at[1, p])
-        got(dw.at[cols(1 - c, hidden), pl.ds(p * part, part)], w_r.at[2, p])
-    got(shtab.at[DB], sh_r.at[2])
+    down_ready(1)
+    down_ready(2)
+    got(shtab.at[DB], sh_r.at[1])
     for block in range(4):
         line = jnp.sum(jnp.where(expert_id == e, shtab[block], 0.0), axis=0, keepdims=True)
         column = jnp.broadcast_to(line, (128, rows)).T
         for h in range(2):
             shcol[pl.ds(base(block, h), half), :] = column[h * half : (h + 1) * half]
-    expert_chunk(XB, nears[0], False, 3)
+    EARLY, LATE, FAR = rows, 2 * rows, 3 * rows
+
+    paired_sides(0, nears[0])
+    expert_rows(EARLY, rows, nears[0], wide)
+    side_arrival(nears[2], 0)
+    paired_sides(0, nears[1])
+    expert_rows(EARLY, rows, nears[1], wide)
     at_middle(lambda: z_arrival(1, nears[2], 1))
     at_edge(lambda: arrivals(1, 1))
-    side_arrival(nears[1], 0)
-    side_arrival(nears[1], 1)
-    EARLY, X_LATE, Y_LATE, FAR = rows + half, rows, 2 * rows + half, 3 * rows
-    expert_rows(XB * rows, 3 * rows, 2 * nears[1] + c, part)
-    paired(DB, nears[1])
-    for i in range(2):
-        for order in range(2):
-            paired_half(i, order, nears[1])
-    expert_rows(XB * rows, 3 * rows, 2 * nears[1] + 1 - c, part)
-    side_arrival(nears[2], 0)
     expert_rows(EARLY, rows, 2 * nears[2] + c, part)
-    paired_half(0, 0, nears[2])
-    paired_half(1, 0, nears[2])
+    paired_sides(0, nears[2])
     expert_rows(EARLY, rows, 2 * nears[2] + 1 - c, part)
     expert_activate(EARLY, rows, 1)
-    at_edge(lambda: arrivals(1, 2))
-    side_arrival(nears[2], 1)
+    side_arrival(nears[0], 1)
+    paired(DB, nears[0])
+    expert_rows(FAR, rows, nears[0], wide)
 
     def down(start, count, p):
         span = pl.ds(start, count)
@@ -878,13 +873,13 @@
         return carry
 
     top, rest = pl.ds(0, half), pl.ds(half, half)
-    sides = ((0, X_LATE, 0, 1, xn), (1, Y_LATE, 1, 0, yn))
+    sides = ((0, XB, 0, 1, xn), (1, YB, 1, 0, yn))
 
     def far_share(j):
         span = cols(fars[j], part)
         dsend[:, span] = low(down(FAR, rows, fars[j]))
-        remote(dsend.at[top, span], din.at[0, :, span], d_s.at[0, j], d_r.at[0, j], xn)
-        remote(dsend.at[rest, span], din.at[1, :, span], d_s.at[1, j], d_r.at[1, j], yn)
+        remote(dsend.at[top, span], din.at[0, :, span], d_s.at[0], d_r.at[j], xn)
+        remote(dsend.at[rest, span], din.at[1, :, span], d_s.at[1], d_r.at[j], yn)
 
     def early_share(j):
         span = cols(fars[j], part)
@@ -892,17 +887,18 @@
         for i, start, now, later, dev in sides:
             esend[i, :, span] = value[i * half : (i + 1) * half]
             target = xyin.at[i, pl.ds(now * half, half), span]
-            remote(esend.at[i, :, span], target, e_s.at[i, 0, j], e_r.at[i, 0, j], dev)
+            remote(esend.at[i, :, span], target, e_s.at[i, 0], e_r.at[j], dev)
 
     def late_share(j):
         span = cols(fars[j], part)
+        value = down(LATE, rows, fars[j])
+        for i in range(2):
+            late[i] = value[i * half : (i + 1) * half]
+        got(din.at[:, :, span], d_r.at[j])
         for i, start, now, later, dev in sides:
-            late[i] = down(start, half, fars[j])
-        for i, start, now, later, dev in sides:
-            got(din.at[1 - i, :, span], d_r.at[1 - i, j])
             lsend[i, :, span] = low(late[i] + f32(din[1 - i, :, span]))
             target = xyin.at[i, pl.ds(later * half, half), span]
-            remote(lsend.at[i, :, span], target, e_s.at[i, 1, j], e_r.at[i, 1, j], dev)
+            remote(lsend.at[i, :, span], target, e_s.at[i, 1], e_r.at[j], dev)
 
     def total(j):
         span = cols(fars[j], part)
@@ -910,9 +906,7 @@
 
     def total_ready(j):
         span = cols(fars[j], part)
-        for i, start, now, later, dev in sides:
-            got(xyin.at[i, pl.ds(now * half, half), span], e_r.at[i, 0, j])
-            got(xyin.at[i, pl.ds(later * half, half), span], e_r.at[i, 1, j])
+        got(xyin.at[:, :, span], e_r.at[j])
 
     def total_half(j, h):
         z_send(1, j, fars[j], h, total(j))
@@ -922,31 +916,38 @@
         total_half(j, 0)
         total_half(j, 1)
 
-    expert_rows(Y_LATE, half + rows, 2 * nears[2] + c, part)
     expert_hidden(EARLY, rows, 1)
     early_share(0)
     early_share(1)
+    expert_rows(FAR, rows, 2 * nears[1] + c, part)
+    paired(DB, nears[1])
+    expert_rows(FAR, rows, 2 * nears[1] + 1 - c, part)
+    at_edge(lambda: arrivals(1, 2))
+    expert_rows(FAR, rows, 2 * nears[2] + c, part)
+    side_arrival(nears[1], 1)
+    paired_sides(1, nears[0])
+    expert_rows(LATE, rows, nears[0], wide)
+    side_arrival(nears[2], 1)
     paired(DB, nears[2])
-    paired_half(1, 1, nears[2])
-    expert_rows(Y_LATE, half + rows, 2 * nears[2] + 1 - c, part)
+    expert_rows(FAR, rows, 2 * nears[2] + 1 - c, part)
     expert_activate(FAR, rows, 2)
-    expert_activate(Y_LATE, half, 4)
-    expert_rows(X_LATE, half, 2 * nears[2] + c, part)
-    paired_half(0, 1, nears[2])
-    expert_rows(X_LATE, half, 2 * nears[2] + 1 - c, part)
-    expert_activate(X_LATE, half, 3)
+    paired_sides(1, nears[1])
+    expert_rows(LATE, rows, nears[1], wide)
     expert_hidden(FAR, rows, 2)
     far_share(0)
     far_share(1)
+    expert_rows(LATE, rows, 2 * nears[2] + c, part)
+    paired_sides(1, nears[2])
+    expert_rows(LATE, rows, 2 * nears[2] + 1 - c, part)
+    expert_activate(LATE, rows, 3)
     at_middle(lambda: mixer_send(0))
     expert_hidden(0, rows, 0)
-    got(shid.at[:, cols(1 - c, shared)], h_r.at[5])
+    got(shid.at[:, cols(1 - c, shared)], h_r.at[4])
     lax.fori_loop(0, chips, own_down, 0)
-    expert_hidden(X_LATE, half, 3)
-    expert_hidden(Y_LATE, half, 4)
+    expert_hidden(LATE, rows, 3)
     late_share(0)
+    far_share(2)
     at_middle(lambda: mixer_send(1))
-    far_share(2)
     late_share(1)
     early_share(2)
     at_middle(lambda: mixer_send(2))
@@ -979,47 +980,35 @@
     routed_out = pltpu.make_async_copy(out_ref, out_hbm, in_l.at[8])
     routed_out.start()
 
-    for kind, block in ((0, OWN), (1, DB)):
+    for kind in range(2):
         for s in range(chips):
 
-            @pl.when(has_r & (s <= z))
+            @pl.when((has_r & (s <= z)) | (has_l & (s > z)))
             def _():
                 for h in range(2):
-                    sent(halved(block, s, h), ag_s.at[kind, 0, s, h])
-
-            @pl.when(has_l & (s >= z))
-            def _():
-                for h in range(2):
-                    sent(halved(block, s, h), ag_s.at[kind, 1, s, h])
-
-    for s in range(chips):
-        for i in range(2):
-            for order in range(2):
-                sent(halved(OWN, s, 0), xy_s.at[i, s, order])
-                sent(halved(OWN, s, 0), pt_s.at[(XB, YB)[i], s, order])
-        for block in (OWN, DB):
-            sent(piece(block, s, c), pt_s.at[block, s, 0])
+                    sent(halved(OWN, s, h), ag_s.at[kind, s, h])
+
+        @pl.when(has_l)
+        def _():
+            for h in range(2):
+                sent(halved(OWN, z, h), ag_s.at[kind, chips, h])
+
     for i in range(2):
-        sent(halved(DB, z, i), dr_s.at[i])
-        sent(kv_rows(OWN, 0, rows), kv_s.at[i])
-        sent(kv_rows(OWN, 0, half), kv_s.at[2 + i])
+        sent(dsend, xy_s.at[i])
+        sent(dsend.at[top], d_s.at[i])
+        sent(esend.at[i], e_s.at[i, 0])
+        sent(lsend.at[i], e_s.at[i, 1])
+        sent(zout.at[i], z_s.at[i])
     for i in range(3):
-        sent(shtab.at[OWN], sh_s.at[i])
-        for p in range(chips):
-            src, dst, depth = downs[i]
-            sent(dst.at[cols(c, depth), pl.ds(p * part, part)], w_s.at[i, p])
-    for count, index in ((rows, 0), (rows, 1), (rows, 2), (half, 3), (half, 4)):
-        sent(hid.at[pl.ds(0, count), cols(c, hidden)], h_s.at[index])
-    sent(shid.at[:, cols(c, shared)], h_s.at[5])
-    sent(ho.at[:, cols(c, vwide)], h_s.at[6])
-    for i in range(2):
-        for j in range(chips):
-            sent(dsend.at[top, pl.ds(j * part, part)], d_s.at[i, j])
-            sent(esend.at[i, :, pl.ds(j * part, part)], e_s.at[i, 0, j])
-            sent(lsend.at[i, :, pl.ds(j * part, part)], e_s.at[i, 1, j])
-        for j in range(chips - 1):
-            for h in range(2):
-                sent(zout.at[i, j, pl.ds(0, half)], z_s.at[i, j, h])
+        src, dst, depth = downs[i]
+        sent(dst.at[cols(c, depth), :], w_s.at[i])
+    sent(xall.at[pl.ds(0, 2 * rows), :], pt_s.at[0])
+    sent(piece(DB, z, c), dr_s.at[0])
+    sent(kv_rows(OWN, 0, 3 * rows), kv_s.at[0])
+    sent(shtab.at[pl.ds(OWN, 3)], sh_s.at[0])
+    sent(hid.at[:, cols(c, hidden)], h_s.at[0])
+    sent(shid.at[:, cols(c, shared)], h_s.at[1])
+    sent(ho.at[:, cols(c, vwide)], h_s.at[2])
     mix_out.wait()
     routed_out.wait()
 
@@ -1126,28 +1115,28 @@
             pltpu.VMEM((rows, 2 * vwide), BF16),
             pltpu.VMEM((groups, 8, rows), F32),
             pltpu.VMEM((groups * rows, 128), F32),
-            dma((5 + 3 * chips,)),
-            dma((3, chips)),
-            dma((3, chips)),
-            dma((2, 2, chips, 2)),
-            dma((2, chips, 2)),
-            dma((2, chips, 2)),
+            dma((8,)),
+            dma((3,)),
+            dma((3,)),
+            dma((2, chips + 1, 2)),
             dma((2, chips, 2)),
             dma((2,)),
+            dma((2, chips)),
+            dma((1,)),
+            dma((1,)),
+            dma((1,)),
+            dma((4, chips)),
+            dma((1,)),
             dma((2,)),
-            dma((4, chips, 2)),
-            dma((4, chips, 2)),
-            dma((4,)),
-            dma((4,)),
+            dma((1,)),
+            dma((2,)),
             dma((3,)),
-            dma((3,)),
-            dma((7,)),
-            dma((7,)),
-            dma((2, chips)),
-            dma((2, chips)),
-            dma((2, 2, chips)),
-            dma((2, 2, chips)),
-            dma((2, chips - 1, 2)),
+            dma((6,)),
+            dma((2,)),
+            dma((chips,)),
+            dma((2, 2)),
+            dma((chips,)),
+            dma((2,)),
             dma((2, chips + 1, 2)),
             dma((9,)),
         ],

time: 84.9 us -> 79.8 us (0.940)
  Pallas kernels: 84 us -> 78.8 us
    pallas_call x1, Pallas kernels: 82.2 us -> 77 us  [kernel_body(): pl.pallas_call(functools.partial(layer_kernel, chips), out_shape=(out, ou...]
where the time goes in v4:
time: 79.8 us; the launch traced here: 79.6 us
  Pallas kernels  78.8 us (99%)
  between operations  0.8 us (1%)
    pallas_call x1, Pallas kernels, kernel_body(): pl.pallas_call(functools.partial(layer_kernel, chips), out_shape=(out, ou...  77 us
    pallas_call x1, Pallas kernels, kernel_body(): pl.pallas_call(emit_kernel, out_shape=(out, out), in_specs=[hbm, hbm], ou...  1.77 us

profile of v4, /device:TPU:0, one launch (start us, length us, event | category | flops | bytes accessed | tf_op | source)
XLA Modules:
  0.0 79.6 jit_solution(4346370539152340371)
XLA Ops:
  0.6 77.0 %layer.1 = (bf16[256,512]{1,0:T(8,128)(2,1)}, bf16[256,512]{1,0:T(8,128)(2,1)}) custom-call(f32[2]{0:T(128)} %lam_ref.1, bf16[256,256]{1,0:T(8,128)(2,1)} %q_hbm.1, bf16[256,256]{1,0:T(8,128)(2,1)} %k_hbm.1, bf16[256,256]{1,0:T(8,128)(2,1)} %v_hbm.1, f32[1,128]{1,0:T(1,128)} %bitcast.11, bf16[256,512]{1,0:T(8,128)(2,1)} %x_hbm.1, s32[2,256]{1,0:T(2,128)} %bitcast.9, ...), custom_call_target="tpu_custom_call" | custom-call | tf_op jit(solution)/shard_map/layer/pallas_call | solution.py:1072
  77.7 1.8 %emit.1 = (bf16[256,512]{1,0:T(8,128)(2,1)}, bf16[256,512]{1,0:T(8,128)(2,1)}) custom-call(bf16[256,512]{1,0:T(8,128)(2,1)} %get-tuple-element.4.mixed_hbm, bf16[256,512]{1,0:T(8,128)(2,1)} %get-tuple-element.5.routed_hbm), custom_call_target="tpu_custom_call" | custom-call | tf_op jit(solution)/shard_map/emit/pallas_call | solution.py:1165

commit v5 on v4

--- a/solution.py
+++ b/solution.py
@@ -294,8 +294,6 @@
     sg_hbm,
     su_hbm,
     sd_hbm,
-    mix_hbm,
-    out_hbm,
     mix_ref,
     out_ref,
     xall,
@@ -401,6 +399,11 @@
     def cols(index, width):
         return pl.ds(pl.multiple_of(index * width, width), width)
 
+    own_rows = pl.ds(0, rows)
+    own_x = pltpu.make_async_copy(
+        x_hbm, xall.at[own_rows, pl.ds(pl.multiple_of(t * part, part), part)], in_l.at[0]
+    )
+    own_x.start()
     barrier = pltpu.get_barrier_semaphore()
     for dev in (pt, xn, yn):
         pl.semaphore_signal(barrier, inc=1, device_id=dev, device_id_type=MESH)
@@ -430,9 +433,8 @@
                     w_l.at[5 + i],
                 )
             )
-    own_rows = pl.ds(0, rows)
     inputs = [
-        pltpu.make_async_copy(x_hbm, xall.at[own_rows, cols(t, part)], in_l.at[0]),
+        own_x,
         pltpu.make_async_copy(q_hbm, q_ref, in_l.at[1]),
         pltpu.make_async_copy(k_hbm, k_ref, in_l.at[2]),
         pltpu.make_async_copy(v_hbm, kv.at[own_rows, pl.ds(kwide, vwide)], in_l.at[3]),
@@ -440,7 +442,6 @@
         pltpu.make_async_copy(rw_hbm, rw_ref, in_l.at[5]),
         pltpu.make_async_copy(gain_hbm, gain_ref, in_l.at[6]),
     ]
-    inputs[0].start()
     inputs[1].start()
     inputs[2].start()
     loads[4].start()
@@ -460,14 +461,14 @@
     def halved(block, s, h, core=None):
         return xall.at[pl.ds(base(block, h), half), cols(2 * s + (c if core is None else core), part)]
 
-    def z_forward(src, kind, block, s, h, right, left, slot=None):
+    def z_forward(src, kind, block, s, h, right, left):
         @pl.when(right)
         def _():
-            remote(src, halved(block, s, h), ag_s.at[kind, s, h], ag_r.at[kind, s, h], zr)
+            remote(src, halved(block, s, h), ag_s.at[0], ag_r.at[kind, s, h], zr)
 
         @pl.when(left)
         def _():
-            remote(src, halved(block, s, h), ag_s.at[kind, s if slot is None else slot, h], ag_r.at[kind, s, h], zl)
+            remote(src, halved(block, s, h), ag_s.at[0], ag_r.at[kind, s, h], zl)
 
     def to_pair(src, block, s):
         remote(src, piece(block, s, c), pt_s.at[0], pt_r.at[block, s], pt)
@@ -507,7 +508,7 @@
     pl.semaphore_wait(barrier, 3 + has_r.astype(jnp.int32) + has_l.astype(jnp.int32))
 
     for h in range(2):
-        z_forward(halved(OWN, z, h), 0, OWN, z, h, has_r, has_l, chips)
+        z_forward(halved(OWN, z, h), 0, OWN, z, h, has_r, has_l)
     own_half(0, 0)
     own_half(1, 0)
     to_pair(piece(OWN, z, c), OWN, z)
@@ -741,7 +742,7 @@
     at_edge(lambda: to_xy(nears[1], 0))
     got(piece(DB, z, c), dr_r.at[0])
     for h in range(2):
-        z_forward(halved(DB, z, h), 1, DB, z, h, has_r, has_l, chips)
+        z_forward(halved(DB, z, h), 1, DB, z, h, has_r, has_l)
     to_pair(piece(DB, z, c), DB, z)
     give_down(0)
     attend_first(2)
@@ -973,26 +974,11 @@
     late_share(3)
     at_middle(middle_second)
     z_finish(0, lambda at: macc[at, cols(z, part)])
-    mix_out = pltpu.make_async_copy(mix_ref, mix_hbm, in_l.at[7])
-    mix_out.start()
     total_ready(3)
     z_finish(1, total(3))
-    routed_out = pltpu.make_async_copy(out_ref, out_hbm, in_l.at[8])
-    routed_out.start()
-
-    for kind in range(2):
-        for s in range(chips):
-
-            @pl.when((has_r & (s <= z)) | (has_l & (s > z)))
-            def _():
-                for h in range(2):
-                    sent(halved(OWN, s, h), ag_s.at[kind, s, h])
-
-        @pl.when(has_l)
-        def _():
-            for h in range(2):
-                sent(halved(OWN, z, h), ag_s.at[kind, chips, h])
-
+
+    at_middle(lambda: sent(zin, ag_s.at[0]))
+    at_edge(lambda: sent(zin.at[0, pl.ds(0, 2)], ag_s.at[0]))
     for i in range(2):
         sent(dsend, xy_s.at[i])
         sent(dsend.at[top], d_s.at[i])
@@ -1009,18 +995,14 @@
     sent(hid.at[:, cols(c, hidden)], h_s.at[0])
     sent(shid.at[:, cols(c, shared)], h_s.at[1])
     sent(ho.at[:, cols(c, vwide)], h_s.at[2])
-    mix_out.wait()
-    routed_out.wait()
-
-
-def emit_kernel(mixed_hbm, routed_hbm, mix_hbm, out_hbm, mixed, routed, sems):
-    pairs = ((mixed_hbm, mixed, mix_hbm), (routed_hbm, routed, out_hbm))
-    loads = [pltpu.make_async_copy(src, held, sems.at[i]) for i, (src, held, _) in enumerate(pairs)]
-    stores = [pltpu.make_async_copy(held, dst, sems.at[2 + i]) for i, (_, held, dst) in enumerate(pairs)]
-    for load in loads:
-        load.start()
-    for load, store in zip(loads, stores):
-        load.wait()
+
+
+def emit_kernel(mixed, routed, mix_hbm, out_hbm, sems):
+    stores = [
+        pltpu.make_async_copy(mixed, mix_hbm, sems.at[0]),
+        pltpu.make_async_copy(routed, out_hbm, sems.at[1]),
+    ]
+    for store in stores:
         store.start()
     for store in stores:
         store.wait()
@@ -1069,14 +1051,14 @@
     hbm = pl.BlockSpec(memory_space=pl.ANY)
     dma = pltpu.SemaphoreType.DMA
     out = jax.ShapeDtypeStruct((rows, part), BF16)
+    held = pltpu.VMEM((rows, part), BF16)
+    vmem = pl.BlockSpec(memory_space=pltpu.VMEM)
     mixed, routed = pl.pallas_call(
         functools.partial(layer_kernel, chips),
-        out_shape=(out, out),
+        out_shape=(held, held),
         in_specs=[smem] + [hbm] * 15,
-        out_specs=(hbm, hbm),
+        out_specs=(vmem, vmem),
         scratch_shapes=[
-            pltpu.VMEM((rows, part), BF16),
-            pltpu.VMEM((rows, part), BF16),
             pltpu.VMEM((groups * rows, width), BF16),
             pltpu.VMEM((width, 2 * hidden), BF16),
             pltpu.VMEM((2 * hidden, mine), BF16),
@@ -1118,7 +1100,7 @@
             dma((8,)),
             dma((3,)),
             dma((3,)),
-            dma((2, chips + 1, 2)),
+            dma((1,)),
             dma((2, chips, 2)),
             dma((2,)),
             dma((2, chips)),
@@ -1138,10 +1120,10 @@
             dma((chips,)),
             dma((2,)),
             dma((2, chips + 1, 2)),
-            dma((9,)),
+            dma((7,)),
         ],
         compiler_params=pltpu.CompilerParams(
-            collective_id=0, has_side_effects=True, vmem_limit_bytes=67043328
+            collective_id=0, has_side_effects=True, vmem_limit_bytes=61865984
         ),
         name="layer",
     )(
@@ -1165,9 +1147,10 @@
     return pl.pallas_call(
         emit_kernel,
         out_shape=(out, out),
-        in_specs=[hbm, hbm],
+        in_specs=[vmem, vmem],
         out_specs=(hbm, hbm),
-        scratch_shapes=[pltpu.VMEM((rows, part), BF16), pltpu.VMEM((rows, part), BF16), dma((4,))],
+        scratch_shapes=[dma((2,))],
+        compiler_params=pltpu.CompilerParams(vmem_limit_bytes=1 << 20),
         name="emit",
     )(mixed, routed)
 

time: 79.8 us -> 77.9 us (0.976)
  Pallas kernels: 78.8 us -> 77 us
    pallas_call x2, Pallas kernels: 78.8 us -> 77 us  [the longest x1 76.2 us: kernel_body(): pl.pallas_call(functools.partial(layer_kernel, chips), out_shape=(held, h...]
where the time goes in v5:
time: 77.9 us; the launch traced here: 77.8 us
  Pallas kernels  77 us (99%)
  between operations  0.8 us (1%)
    pallas_call x1, Pallas kernels, kernel_body(): pl.pallas_call(functools.partial(layer_kernel, chips), out_shape=(held, h...  76.2 us

profile of v5, /device:TPU:0, one launch (start us, length us, event | category | flops | bytes accessed | tf_op | source)
XLA Modules:
  0.0 77.8 jit_solution(6017256325358309301)
XLA Ops:
  0.6 76.2 %layer.1 = (bf16[256,512]{1,0:T(8,128)(2,1)S(1)}, bf16[256,512]{1,0:T(8,128)(2,1)S(1)}) custom-call(f32[2]{0:T(128)} %lam_ref.1, bf16[256,256]{1,0:T(8,128)(2,1)} %q_hbm.1, bf16[256,256]{1,0:T(8,128)(2,1)} %k_hbm.1, bf16[256,256]{1,0:T(8,128)(2,1)} %v_hbm.1, f32[1,128]{1,0:T(1,128)} %bitcast.11, bf16[256,512]{1,0:T(8,128)(2,1)} %x_hbm.1, s32[2,256]{1,0:T(2,128)} %bitcast.9, ...), custom_call_target="tpu_custom_call" | custom-call | tf_op jit(solution)/shard_map/layer/pallas_call | solution.py:1056
  76.8 0.8 %emit.1 = (bf16[256,512]{1,0:T(8,128)(2,1)}, bf16[256,512]{1,0:T(8,128)(2,1)}) custom-call(bf16[256,512]{1,0:T(8,128)(2,1)S(1)} %get-tuple-element.4.mixed, bf16[256,512]{1,0:T(8,128)(2,1)S(1)} %get-tuple-element.5.routed), custom_call_target="tpu_custom_call" | custom-call | tf_op jit(solution)/shard_map/emit/pallas_call | solution.py:1147

commit v6 on v5

--- a/solution.py
+++ b/solution.py
@@ -919,24 +919,22 @@
 
     expert_hidden(EARLY, rows, 1)
     early_share(0)
+    expert_chunk(DB, nears[1], False)
+    at_edge(lambda: arrivals(1, 2))
+    side_arrival(nears[1], 1)
     early_share(1)
-    expert_rows(FAR, rows, 2 * nears[1] + c, part)
-    paired(DB, nears[1])
-    expert_rows(FAR, rows, 2 * nears[1] + 1 - c, part)
-    at_edge(lambda: arrivals(1, 2))
     expert_rows(FAR, rows, 2 * nears[2] + c, part)
-    side_arrival(nears[1], 1)
-    paired_sides(1, nears[0])
-    expert_rows(LATE, rows, nears[0], wide)
     side_arrival(nears[2], 1)
     paired(DB, nears[2])
     expert_rows(FAR, rows, 2 * nears[2] + 1 - c, part)
     expert_activate(FAR, rows, 2)
-    paired_sides(1, nears[1])
-    expert_rows(LATE, rows, nears[1], wide)
+    paired_sides(1, nears[0])
+    expert_rows(LATE, rows, nears[0], wide)
     expert_hidden(FAR, rows, 2)
     far_share(0)
     far_share(1)
+    paired_sides(1, nears[1])
+    expert_rows(LATE, rows, nears[1], wide)
     expert_rows(LATE, rows, 2 * nears[2] + c, part)
     paired_sides(1, nears[2])
     expert_rows(LATE, rows, 2 * nears[2] + 1 - c, part)

time: 77.9 us -> 77.6 us (level)
  no operation moved by 1% of the time
where the time goes in v6:
time: 77.6 us; the launch traced here: 77.4 us
  Pallas kernels  76.6 us (99%)
  between operations  0.8 us (1%)
    pallas_call x1, Pallas kernels, kernel_body(): pl.pallas_call(functools.partial(layer_kernel, chips), out_shape=(held, h...  75.8 us

profile of v6, /device:TPU:0, one launch (start us, length us, event | category | flops | bytes accessed | tf_op | source)
XLA Modules:
  0.0 77.4 jit_solution(15348780012973714873)
XLA Ops:
  0.6 75.8 %layer.1 = (bf16[256,512]{1,0:T(8,128)(2,1)S(1)}, bf16[256,512]{1,0:T(8,128)(2,1)S(1)}) custom-call(f32[2]{0:T(128)} %lam_ref.1, bf16[256,256]{1,0:T(8,128)(2,1)} %q_hbm.1, bf16[256,256]{1,0:T(8,128)(2,1)} %k_hbm.1, bf16[256,256]{1,0:T(8,128)(2,1)} %v_hbm.1, f32[1,128]{1,0:T(1,128)} %bitcast.11, bf16[256,512]{1,0:T(8,128)(2,1)} %x_hbm.1, s32[2,256]{1,0:T(2,128)} %bitcast.9, ...), custom_call_target="tpu_custom_call" | custom-call | tf_op jit(solution)/shard_map/layer/pallas_call | solution.py:1054
  76.5 0.8 %emit.1 = (bf16[256,512]{1,0:T(8,128)(2,1)}, bf16[256,512]{1,0:T(8,128)(2,1)}) custom-call(bf16[256,512]{1,0:T(8,128)(2,1)S(1)} %get-tuple-element.4.mixed, bf16[256,512]{1,0:T(8,128)(2,1)S(1)} %get-tuple-element.5.routed), custom_call_target="tpu_custom_call" | custom-call | tf_op jit(solution)/shard_map/emit/pallas_call | solution.py:1145
